TPU v7x, 32 devices: a whole 2x2x4 slice. The times are simulated.
32 devices in a mesh: sp: 8 (over z, y), tp: 4 (over x, core).
Axes of the slice: x: 2, y: 2, z: 4, core: 2. Of those that a mesh axis runs over, the one named last changes fastest.
Arguments:
- query_rows: bfloat16 [2048, 2048], P('sp', 'tp'), may hold values from -5.5 to 5.5
- key_rows: bfloat16 [2048, 2048], P('sp', 'tp'), may hold values from -5.5 to 5.5
- value_rows: bfloat16 [2048, 2048], P('sp', 'tp'), may hold values from -6 to 6
- out_grad: bfloat16 [2048, 2048], P('sp', 'tp'), may hold values from -96 to 96
- rel_bias: float32 [256, 32], replicated, may hold values from -3 to 3
Outputs:
- query_grad: bfloat16 [2048, 2048], P('sp', 'tp')
- key_grad: bfloat16 [2048, 2048], P('sp', 'tp')
- value_grad: bfloat16 [2048, 2048], P('sp', 'tp')
- table_grad: float32 [256, 32], P('sp')
All inputs are finite; a program needn't handle non-finite values.
Results may differ from a plain program's by a relative error of at most 0.007.
Values may be sent and summed in bfloat16 or wider, within the bound.
A program may use at most 64 MiB of HBM per device.

v0:
```python
from functools import partial
import math

import jax
import jax.numpy as jnp
from jax import lax
from jax.experimental import pallas as pl
from jax.experimental.pallas import tpu as pltpu
from jax.sharding import PartitionSpec as P

HEAD_DIM = 64
SEG = 64
LEFT = 4
CLIP = 128

LANES = 2 * HEAD_DIM
REACH = LEFT * SEG
BLK = 2 * SEG
BAND = REACH + BLK
WRAP = 3 * BLK
NEG_FILL = -1e30
LOG2E = math.log2(math.e)
MESH = pl.DeviceIdType.MESH
F32 = jnp.float32
BF16 = jnp.bfloat16

NT = (((1,), (1,)), ((), ()))
NN = (((1,), (0,)), ((), ()))
TN = (((0,), (0,)), ((), ()))


def dot(a, b, dims):
    return lax.dot_general(a, b, dims, preferred_element_type=F32)


def turned(x, amount):
    amount %= x.shape[1]
    return pltpu.roll(x, amount, 1) if amount else x


def row_turned(x, sign):
    row = lax.broadcasted_iota(jnp.int32, x.shape, 0)
    for bit in (1, 2, 4):
        x = jnp.where((row & bit) != 0, turned(x, sign * bit), x)
    return x


def build_bias(table_row, bias_ref, pair, lane):
    last = table_row[:, 2 * CLIP - 1 :]
    flat = jnp.broadcast_to(last, (1, BLK))
    shape = (8, BLK)
    line = jnp.concatenate([table_row[:, CLIP:], flat, table_row[:, :CLIP]], axis=1)
    base = row_turned(jnp.broadcast_to(line, (8, WRAP)), 1)
    query = lax.broadcasted_iota(jnp.int32, shape, 1)
    cols = pl.ds(lane * BLK, BLK)
    flat8 = jnp.broadcast_to(last, shape)
    for group in range(BAND // 8):
        row = group * 8
        if row < BLK:
            tile = flat8
        else:
            sheared = turned(base, row % BLK)
            tile = sheared[:, BLK : 2 * BLK] if row < 2 * BLK else sheared[:, :BLK]
        if row < SEG:
            tile = jnp.where(query >= SEG, NEG_FILL, tile)
        if row >= BAND - SEG:
            tile = jnp.where(query < SEG, NEG_FILL, tile)
        bias_ref[pair, pl.ds(row, 8), cols] = tile


def diagonals(square):
    parts = []
    for group in range(BLK // 8):
        near = square[2 * BLK + group * 8 : 2 * BLK + group * 8 + 8]
        far = square[BLK + group * 8 : BLK + group * 8 + 8]
        parts.append(jnp.concatenate([near, far, jnp.zeros_like(near)], axis=1))
    step = 8
    while len(parts) > 1:
        parts = [a + turned(b, -step) for a, b in zip(parts[::2], parts[1::2])]
        step *= 2
    sums = jnp.sum(row_turned(parts[0], -1), axis=0, keepdims=True)
    return sums, jnp.sum(square[:BLK], axis=0, keepdims=True)


def kernel(
    sp_size, tp_size,
    q_hbm, k_hbm, v_hbm, d_hbm, table_hbm,
    dq_ref, dk_ref, dv_ref, dt_ref,
    qx, dx, k_ref, v_ref, bias_ref, square_ref, grown_ref, dprob_ref,
    own_k, own_v, own_q, back_q, got_q,
    local_stats, right_stats, halo_stats, left_stats,
    table_rows, pieces, piece_got, shares,
    load_sem, seq_send, seq_recv, ls_send, ls_recv, hs_send, hs_recv, back_send, back_recv,
    piece_send, piece_recv, share_send, share_recv,
):
    rows, width = q_hbm.shape
    pairs = width // LANES
    heads = width // HEAD_DIM
    me = lax.axis_index("sp")
    col = lax.axis_index("tp")
    has_left = me > 0
    has_right = me < sp_size - 1
    left = jnp.maximum(me - 1, 0)
    right = jnp.minimum(me + 1, sp_size - 1)

    own = pl.ds(0, rows)
    loads = [
        pltpu.make_async_copy(src, dst, load_sem.at[i])
        for i, (src, dst) in enumerate(
            (
                (k_hbm, k_ref),
                (v_hbm, v_ref),
                (q_hbm, qx.at[own]),
                (d_hbm, dx.at[own]),
                (table_hbm, table_rows),
            )
        )
    ]
    for load in loads:
        load.start()

    barrier = pltpu.get_barrier_semaphore()
    for k in range(1, sp_size):
        pl.semaphore_signal(
            barrier, inc=1, device_id=(lax.rem(me + k, sp_size), col), device_id_type=MESH
        )
    for k in range(1, tp_size):
        pl.semaphore_signal(
            barrier, inc=1, device_id=(me, lax.rem(col + k, tp_size)), device_id_type=MESH
        )
    pl.semaphore_wait(barrier, sp_size - 1 + tp_size - 1)

    def remote(src, dst, send, recv, target):
        return pltpu.make_async_remote_copy(
            src_ref=src,
            dst_ref=dst,
            send_sem=send,
            recv_sem=recv,
            device_id=(target, col),
            device_id_type=MESH,
        )

    def seq_copies(p):
        cols = pl.ds(p * LANES, LANES)
        return [
            remote(
                src.at[:, cols],
                dst.at[pl.ds(rows, rows), cols],
                seq_send.at[p, i],
                seq_recv.at[p, i],
                left,
            )
            for i, (src, dst) in enumerate(((q_hbm, qx), (d_hbm, dx)))
        ]

    def local_copy():
        return remote(local_stats, right_stats, ls_send, ls_recv, left)

    def halo_copy(p):
        return remote(halo_stats.at[p], left_stats.at[p], hs_send.at[p], hs_recv.at[p], right)

    def back_copy(p):
        return remote(back_q.at[p], got_q.at[p], back_send.at[p], back_recv.at[p], right)

    early = (pairs + 1) // 2

    @pl.when(has_left)
    def _():
        for p in range(early):
            for copy in seq_copies(p):
                copy.start()

    local_stats[...] = jnp.zeros(local_stats.shape, F32)
    halo_stats[...] = jnp.zeros(halo_stats.shape, F32)

    @pl.when(jnp.logical_not(has_left))
    def _():
        spot = lax.broadcasted_iota(jnp.int32, left_stats.shape, 1)
        left_stats[...] = jnp.where((spot == 0) | (spot == 3), NEG_FILL, 0.0)

    loads[4].wait()
    for h in range(heads):
        row = table_rows[pl.ds(col * heads + h, 1), :] * LOG2E
        build_bias(row, bias_ref, h // 2, h % 2)

    for load in loads[:4]:
        load.wait()

    low = lax.broadcasted_iota(jnp.int32, (BLK, LANES), 1) < HEAD_DIM
    scale = HEAD_DIM ** -0.5
    sums, tops = [], []

    def split(x):
        zero = jnp.zeros_like(x)
        return jnp.concatenate([jnp.where(low, x, zero), jnp.where(low, zero, x)], axis=0)

    def tile(p, half, halo):
        cols = pl.ds(p * LANES, LANES)
        mine = pl.ds(half * BLK + (rows if halo else 0), BLK)
        start, size, row = (
            (half * BLK, REACH - half * BLK, 0)
            if halo
            else (0, (half + 1) * BLK, REACH - half * BLK)
        )
        keys = pl.ds(start, size)
        qq = split(qx[mine, cols] * jnp.asarray(scale, BF16))
        dd = split(dx[mine, cols])
        return k_ref[keys, cols], v_ref[keys, cols], qq, dd, pl.ds(row, size)

    def partial_softmax(p, half, halo, stats):
        k_blk, v_blk, qq, dd, band = tile(p, half, halo)
        scores = dot(k_blk, qq, NT) * LOG2E + bias_ref[p, band]
        dprobs = dot(v_blk, dd, NT)
        peak = jnp.max(scores, axis=0, keepdims=True)
        grown = jnp.exp2(scores - peak)
        three = (
            peak,
            jnp.sum(grown, axis=0, keepdims=True),
            jnp.sum(grown * dprobs, axis=0, keepdims=True),
        )
        for i, value in enumerate(three):
            stats[p, pl.ds(half * 3 + i, 1), :] = value
        return grown, dprobs

    def tile_grads(p, half, halo, grown, dprobs, stats, others):
        k_blk, v_blk, qq, dd, band = tile(p, half, halo)
        m1, l1, i1 = (stats[p, pl.ds(half * 3 + i, 1), :] for i in range(3))
        m2, l2, i2 = (others[p, pl.ds(half * 3 + i, 1), :] for i in range(3))
        peak = jnp.maximum(m1, m2)
        a1, a2 = jnp.exp2(m1 - peak), jnp.exp2(m2 - peak)
        inverse = 1.0 / (l1 * a1 + l2 * a2)
        inner = (i1 * a1 + i2 * a2) * inverse
        probs = grown * (a1 * inverse)
        dscores = probs * (dprobs - inner)
        ds_half = dscores.astype(BF16)
        flat = dot(k_blk, ds_half, TN)
        both = jnp.concatenate([flat[:HEAD_DIM, :BLK], flat[HEAD_DIM:, BLK:]], axis=0)
        return (
            dscores,
            dot(ds_half, qq, NN),
            dot(probs.astype(BF16), dd, NN),
            jnp.transpose(both) * scale,
        )

    places = (pl.ds(0, BLK), pl.ds(BLK, 2 * BLK))
    for p in range(pairs):
        for half in range(2):
            grown, dprobs = partial_softmax(p, half, False, local_stats)
            grown_ref[p, places[half], :] = grown
            dprob_ref[p, places[half], :] = dprobs

    @pl.when(has_left)
    def _():
        local_copy().start()
        for p in range(early, pairs):
            for copy in seq_copies(p):
                copy.start()

    def halo(p):
        @pl.when(has_right)
        def _():
            for copy in seq_copies(p):
                copy.wait_recv()
            kept = [partial_softmax(p, half, True, halo_stats) for half in range(2)]
            halo_copy(p).start()
            if p == 0:
                local_copy().wait_recv()
            (s0, k0, v0, q0), (s1, k1, v1, q1) = (
                tile_grads(p, half, True, *kept[half], halo_stats, right_stats)
                for half in range(2)
            )
            for ref, a, b in ((own_k, k0, k1), (own_v, v0, v1)):
                ref[p, :BLK, :] = a[:BLK]
                ref[p, BLK:, :] = a[BLK:] + b
            back_q[p, :BLK, :] = q0.astype(BF16)
            back_q[p, BLK:, :] = q1.astype(BF16)
            square_ref[p, :BLK, :] = s0[:BLK] + s1
            square_ref[p, BLK:REACH, :] = s0[BLK:]

        @pl.when(jnp.logical_not(has_right))
        def _():
            own_k[p] = jnp.zeros((rows, LANES), F32)
            own_v[p] = jnp.zeros((rows, LANES), F32)
            square_ref[p, :REACH, :] = jnp.zeros((REACH, 2 * BLK), F32)

    def local(p):
        cols = pl.ds(p * LANES, LANES)

        @pl.when(has_left)
        def _():
            halo_copy(p).wait_recv()

        (s0, k0, v0, q0), (s1, k1, v1, q1) = (
            tile_grads(
                p, half, False,
                grown_ref[p, places[half], :], dprob_ref[p, places[half], :],
                local_stats, left_stats,
            )
            for half in range(2)
        )
        square = jnp.concatenate(
            [
                square_ref[p, :BLK, :],
                square_ref[p, BLK:REACH, :] + s1[:BLK],
                s0 + s1[BLK:],
            ],
            axis=0,
        )
        for lane in range(2):
            s, t = diagonals(square[:, lane * BLK : (lane + 1) * BLK])
            sums.append(s)
            tops.append(t)
        for out, ref, a, b in ((dk_ref, own_k, k0, k1), (dv_ref, own_v, v0, v1)):
            out[:BLK, cols] = (ref[p, :BLK, :] + a + b[:BLK]).astype(BF16)
            out[BLK:, cols] = (ref[p, BLK:, :] + b[BLK:]).astype(BF16)
        own_q[p, :BLK, :] = q0
        own_q[p, BLK:, :] = q1

    lag = pairs
    for p in range(pairs + lag):
        if p < pairs:
            halo(p)
        if p >= lag:
            local(p - lag)

    y = jnp.concatenate(sums, axis=0)
    beyond = jnp.sum(
        y[:, BLK : 2 * BLK] + jnp.concatenate(tops, axis=0), axis=1, keepdims=True
    )
    spot = lax.broadcasted_iota(jnp.int32, (heads, BLK), 1)
    upper = y[:, :BLK] + jnp.where(spot == BLK - 1, beyond, 0.0)
    grad_rows = jnp.concatenate([y[:, 2 * BLK :], upper], axis=1)
    part = 2 * CLIP // sp_size
    for s in range(sp_size):
        pieces[s] = turned(grad_rows, -part * s)[:, :BLK]

    def piece_copy(k):
        target = lax.rem(me + k, sp_size)
        return pltpu.make_async_remote_copy(
            src_ref=pieces.at[target],
            dst_ref=piece_got.at[k - 1],
            send_sem=piece_send.at[k - 1],
            recv_sem=piece_recv.at[k - 1],
            device_id=(target, col),
            device_id_type=MESH,
        )

    def share_copy(k):
        return pltpu.make_async_remote_copy(
            src_ref=shares.at[col],
            dst_ref=shares.at[col],
            send_sem=share_send.at[k - 1],
            recv_sem=share_recv.at[k - 1],
            device_id=(me, lax.rem(col + k, tp_size)),
            device_id_type=MESH,
        )

    def share_arrival(k):
        source = lax.rem(col + tp_size - k, tp_size)
        return pltpu.make_async_remote_copy(
            src_ref=shares.at[source],
            dst_ref=shares.at[source],
            send_sem=share_send.at[k - 1],
            recv_sem=share_recv.at[k - 1],
            device_id=(me, source),
            device_id_type=MESH,
        )

    for k in range(1, sp_size):
        piece_copy(k).start()

    @pl.when(has_right)
    def _():
        for p in range(pairs):
            back_copy(p).start()

    def finish(p):
        cols = pl.ds(p * LANES, LANES)

        @pl.when(has_left)
        def _():
            back_copy(p).wait_recv()
            dq_ref[:, cols] = (own_q[p] + got_q[p].astype(F32)).astype(BF16)

        @pl.when(jnp.logical_not(has_left))
        def _():
            dq_ref[:, cols] = own_q[p].astype(BF16)

    total = pieces[me]
    for k in range(1, sp_size):
        piece_copy(k).wait_recv()
        total = total + piece_got[k - 1]
    shares[col] = total
    for k in range(1, tp_size):
        share_copy(k).start()
    for p in range(pairs):
        finish(p)
    for k in range(1, tp_size):
        share_arrival(k).wait_recv()
    stacked = jnp.concatenate([shares[t] for t in range(tp_size)], axis=0)
    dt_ref[...] = jnp.transpose(stacked)[:part]

    for k in range(1, sp_size):
        piece_copy(k).wait_send()
    for k in range(1, tp_size):
        share_copy(k).wait_send()

    @pl.when(has_left)
    def _():
        local_copy().wait_send()
        for p in range(pairs):
            for copy in seq_copies(p):
                copy.wait_send()

    @pl.when(has_right)
    def _():
        for p in range(pairs):
            halo_copy(p).wait_send()
            back_copy(p).wait_send()


def shards(sp_size, tp_size, query_rows, key_rows, value_rows, out_grad, rel_bias):
    rows, width = query_rows.shape
    pairs = width // LANES
    heads = width // HEAD_DIM
    part = 2 * CLIP // sp_size
    assert rows == REACH and REACH == 2 * BLK and CLIP == BLK
    like = jax.ShapeDtypeStruct((rows, width), BF16)
    dma = pltpu.SemaphoreType.DMA
    shapes = (like, like, like, jax.ShapeDtypeStruct((part, heads * tp_size), F32))
    results = pl.pallas_call(
        partial(kernel, sp_size, tp_size),
        out_shape=shapes,
        in_specs=[pl.BlockSpec(memory_space=pltpu.HBM)] * 5,
        out_specs=tuple([pl.BlockSpec(memory_space=pltpu.VMEM)] * 4),
        scratch_shapes=[
            pltpu.VMEM((2 * rows, width), BF16),
            pltpu.VMEM((2 * rows, width), BF16),
            pltpu.VMEM((rows, width), BF16),
            pltpu.VMEM((rows, width), BF16),
            pltpu.VMEM((pairs, BAND, 2 * BLK), F32),
            pltpu.VMEM((pairs, REACH, 2 * BLK), F32),
            pltpu.VMEM((pairs, BAND, 2 * BLK), F32),
            pltpu.VMEM((pairs, BAND, 2 * BLK), F32),
            pltpu.VMEM((pairs, rows, LANES), F32),
            pltpu.VMEM((pairs, rows, LANES), F32),
            pltpu.VMEM((pairs, rows, LANES), F32),
            pltpu.VMEM((pairs, rows, LANES), BF16),
            pltpu.VMEM((pairs, rows, LANES), BF16),
            pltpu.VMEM((pairs, 8, 2 * BLK), F32),
            pltpu.VMEM((pairs, 8, 2 * BLK), F32),
            pltpu.VMEM((pairs, 8, 2 * BLK), F32),
            pltpu.VMEM((pairs, 8, 2 * BLK), F32),
            pltpu.VMEM(rel_bias.shape[::-1], F32),
            pltpu.VMEM((sp_size, heads, BLK), F32),
            pltpu.VMEM((sp_size - 1, heads, BLK), F32),
            pltpu.VMEM((tp_size, heads, BLK), F32),
            dma((5,)),
            dma((pairs, 2)),
            dma((pairs, 2)),
            dma,
            dma,
            dma((pairs,)),
            dma((pairs,)),
            dma((pairs,)),
            dma((pairs,)),
            dma((sp_size - 1,)),
            dma((sp_size - 1,)),
            dma((tp_size - 1,)),
            dma((tp_size - 1,)),
        ],
        compiler_params=pltpu.CompilerParams(
            collective_id=0, has_side_effects=True, vmem_limit_bytes=48 * 1024 * 1024
        ),
    )(*[pltpu.with_memory_space_constraint(x, pltpu.HBM) for x in (query_rows, key_rows, value_rows, out_grad, jnp.transpose(rel_bias))])
    return pl.pallas_call(
        write_out,
        out_shape=shapes,
        in_specs=[pl.BlockSpec(memory_space=pl.ANY)] * 4,
        out_specs=tuple([pl.BlockSpec(memory_space=pltpu.HBM)] * 4),
        scratch_shapes=[dma((4,))],
        compiler_params=pltpu.CompilerParams(vmem_limit_bytes=1024 * 1024),
    )(*results)


def write_out(*refs):
    sem = refs[-1]
    copies = [pltpu.make_async_copy(refs[i], refs[4 + i], sem.at[i]) for i in range(4)]
    for copy in copies:
        copy.start()
    for copy in copies:
        copy.wait()


def solution(mesh):
    return jax.shard_map(
        partial(shards, mesh.shape["sp"], mesh.shape["tp"]),
        mesh=mesh,
        in_specs=(P("sp", "tp"), P("sp", "tp"), P("sp", "tp"), P("sp", "tp"), P()),
        out_specs=(P("sp", "tp"), P("sp", "tp"), P("sp", "tp"), P("sp", None)),
        check_vma=False,
    )
```

profile of v0, /device:TPU:0, one launch (start us, length us, event | category | flops | bytes accessed | tf_op | source)
XLA Modules:
  0.0 31.9 jit_solution(12682780616451893309)
XLA Ops:
  0.6 30.3 %shard_map.84 = (bf16[256,512]{1,0:T(8,128)(2,1)S(1)}, bf16[256,512]{1,0:T(8,128)(2,1)S(1)}, bf16[256,512]{1,0:T(8,128)(2,1)S(1)}, f32[32,32]{1,0:T(8,128)S(1)}) custom-call(bf16[256,512]{1,0:T(8,128)(2,1)} %q_hbm.1, bf16[256,512]{1,0:T(8,128)(2,1)} %k_hbm.1, bf16[256,512]{1,0:T(8,128)(2,1)} %v_hbm.1, bf16[256,512]{1,0:T(8,128)(2,1)} %d_hbm.1, f32[32,256]{1,0:T(8,128)} %bitcast.1), custom_call_target="tpu_custom_call" | custom-call | tf_op jit(solution)/shard_map/pallas_call | solution.py:431
  31.0 0.9 %shard_map.85 = (bf16[256,512]{1,0:T(8,128)(2,1)}, bf16[256,512]{1,0:T(8,128)(2,1)}, bf16[256,512]{1,0:T(8,128)(2,1)}, f32[32,32]{1,0:T(8,128)}) custom-call(bf16[256,512]{1,0:T(8,128)(2,1)S(1)} %get-tuple-element.8.refs_0_, bf16[256,512]{1,0:T(8,128)(2,1)S(1)} %get-tuple-element.9.refs_1_, bf16[256,512]{1,0:T(8,128)(2,1)S(1)} %get-tuple-element.10.refs_2_, ...), custom_call_target="tpu_custom_call" | custom-call | tf_op jit(solution)/shard_map/pallas_call | solution.py:476
where the time goes:
time: 32.1 us; the launch traced here: 31.9 us
  Pallas kernels  31.3 us (98%)
  between operations  0.64 us (2%)
    pallas_call x1, Pallas kernels, shards(): pl.pallas_call(partial(kernel, sp_size, tp_size), out_shape=shapes, in_sp...  30.3 us
    pallas_call x1, Pallas kernels, shards(): pl.pallas_call(write_out, out_shape=shapes, in_specs=[pl.BlockSpec(memory...  0.91 us

commit v1 on v0

v1 whole, which is shorter than its diff:
```python
from functools import partial
import math

import jax
import jax.numpy as jnp
from jax import lax
from jax.experimental import pallas as pl
from jax.experimental.pallas import tpu as pltpu
from jax.sharding import PartitionSpec as P

HEAD_DIM = 64
SEG = 64
LEFT = 4
CLIP = 128

LANES = 2 * HEAD_DIM
REACH = LEFT * SEG
BLK = 2 * SEG
BAND = REACH + BLK
WRAP = 3 * BLK
NEG_FILL = -1e30
LOG2E = math.log2(math.e)
MESH = pl.DeviceIdType.MESH
F32 = jnp.float32
BF16 = jnp.bfloat16

NT = (((1,), (1,)), ((), ()))
NN = (((1,), (0,)), ((), ()))
TN = (((0,), (0,)), ((), ()))


def dot(a, b, dims):
    return lax.dot_general(a, b, dims, preferred_element_type=F32)


def turned(x, amount):
    amount %= x.shape[1]
    return pltpu.roll(x, amount, 1) if amount else x


def row_turned(x, sign):
    row = lax.broadcasted_iota(jnp.int32, x.shape, 0)
    for bit in (1, 2, 4):
        x = jnp.where((row & bit) != 0, turned(x, sign * bit), x)
    return x


def build_bias(table_row, bias_ref, pair, lane):
    last = table_row[:, 2 * CLIP - 1 :]
    flat = jnp.broadcast_to(last, (1, BLK))
    shape = (8, BLK)
    line = jnp.concatenate([table_row[:, CLIP:], flat, table_row[:, :CLIP]], axis=1)
    base = row_turned(jnp.broadcast_to(line, (8, WRAP)), 1)
    query = lax.broadcasted_iota(jnp.int32, shape, 1)
    cols = pl.ds(lane * BLK, BLK)
    flat8 = jnp.broadcast_to(last, shape)
    for group in range(BAND // 8):
        row = group * 8
        if row < BLK:
            tile = flat8
        else:
            sheared = turned(base, row % BLK)
            tile = sheared[:, BLK : 2 * BLK] if row < 2 * BLK else sheared[:, :BLK]
        if row < SEG:
            tile = jnp.where(query >= SEG, NEG_FILL, tile)
        if row >= BAND - SEG:
            tile = jnp.where(query < SEG, NEG_FILL, tile)
        bias_ref[pair, pl.ds(row, 8), cols] = tile


def diagonals(square):
    parts = []
    for group in range(BLK // 8):
        near = square[2 * BLK + group * 8 : 2 * BLK + group * 8 + 8]
        far = square[BLK + group * 8 : BLK + group * 8 + 8]
        parts.append(jnp.concatenate([near, far, jnp.zeros_like(near)], axis=1))
    step = 8
    while len(parts) > 1:
        parts = [a + turned(b, -step) for a, b in zip(parts[::2], parts[1::2])]
        step *= 2
    sums = jnp.sum(row_turned(parts[0], -1), axis=0, keepdims=True)
    return sums, jnp.sum(square[:BLK], axis=0, keepdims=True)


def kernel(
    sp_size, tp_size, moved,
    q_hbm, k_hbm, v_hbm, d_hbm, table_hbm,
    dq_ref, dk_ref, dv_ref, dt_ref,
    qd, kv, bias_ref, square_ref, grown_ref, dprob_ref, peak_ref,
    own_k, own_v, own_q, back_q, got_q, back_kv, got_kv,
    local_stats, right_stats, halo_stats, left_stats,
    table_rows, pieces, piece_got, shares,
    load_sem, hop_sem, send_sem, seq_recv, back_recv, halo_recv, misc_recv,
):
    rows, width = q_hbm.shape
    pairs = width // LANES
    heads = width // HEAD_DIM
    part = 2 * CLIP // sp_size
    me = lax.axis_index("sp")
    col = lax.axis_index("tp")
    has_left = me > 0
    has_right = me < sp_size - 1
    left = jnp.maximum(me - 1, 0)
    right = jnp.minimum(me + 1, sp_size - 1)
    first, second = pl.ds(0, rows), pl.ds(rows, rows)

    pltpu.make_async_copy(q_hbm, qd.at[0, first], load_sem.at[0]).start()
    pltpu.make_async_copy(d_hbm, qd.at[1, first], load_sem.at[0]).start()
    pltpu.make_async_copy(table_hbm, table_rows, load_sem.at[2]).start()
    pltpu.make_async_copy(k_hbm, kv.at[0, second], load_sem.at[1]).start()
    pltpu.make_async_copy(v_hbm, kv.at[1, second], load_sem.at[1]).start()

    barrier = pltpu.get_barrier_semaphore()

    def greet(sem, step):
        @pl.when(me >= step)
        def _():
            pl.semaphore_signal(sem, inc=1, device_id=(me - step, col), device_id_type=MESH)

        @pl.when(me + step < sp_size)
        def _():
            pl.semaphore_signal(sem, inc=1, device_id=(me + step, col), device_id_type=MESH)

    def greeters(step):
        return (me >= step).astype(jnp.int32) + (me + step < sp_size).astype(jnp.int32)

    greet(barrier, 1)
    for k in range(1, tp_size):
        pl.semaphore_signal(
            barrier, inc=1, device_id=(me, lax.rem(col + k, tp_size)), device_id_type=MESH
        )

    rounds = hop_sem.shape[0]

    def hop(r):
        if 0 < r <= rounds:
            pl.semaphore_wait(hop_sem.at[r - 1], greeters(1 << (r - 1)))
        if r < rounds:
            greet(hop_sem.at[r], 1 << r)

    def remote(src, dst, send, recv, target):
        return pltpu.make_async_remote_copy(
            src_ref=src,
            dst_ref=dst,
            send_sem=send_sem.at[send],
            recv_sem=recv,
            device_id=(target, col),
            device_id_type=MESH,
        )

    def query_copy(start, count):
        cols = pl.ds(start * LANES, count * LANES)
        return remote(
            qd.at[:, first, cols], qd.at[:, second, cols], 0, seq_recv.at[start], left
        )

    def key_copy(p, block):
        cols = pl.ds(p * LANES, LANES)
        return remote(
            kv.at[:, pl.ds(rows + block * BLK, BLK), cols],
            kv.at[:, pl.ds(block * BLK, BLK), cols],
            1,
            seq_recv.at[p + block * (pairs - moved)],
            right,
        )

    def all_keys():
        cols = pl.ds(moved * LANES, width - moved * LANES)
        return remote(kv.at[:, second, cols], kv.at[:, first, cols], 1, misc_recv.at[0], right)

    def local_copy():
        return remote(local_stats, right_stats, 2, misc_recv.at[0], left)

    def halo_copy(p):
        return remote(halo_stats.at[p], left_stats.at[p], 3, halo_recv.at[p], right)

    def back_copy(p):
        return remote(back_q.at[p], got_q.at[p], 4, back_recv.at[p], right)

    def key_back_copy(p):
        i = p - moved
        return remote(back_kv.at[i], got_kv.at[i], 5, back_recv.at[p], left)

    def send_pair(p):
        if p < moved:
            @pl.when(has_left)
            def _():
                query_copy(p, 1).start()
        elif p < pairs:
            @pl.when(has_right)
            def _():
                for block in (1, 0):
                    key_copy(p, block).start()

    def send_back(p):
        if p < moved:
            @pl.when(has_right)
            def _():
                back_copy(p).start()
        else:
            @pl.when(has_left)
            def _():
                key_back_copy(p).start()

    def load_wait(refs, sem):
        pltpu.make_async_copy(refs, refs, sem).wait()

    pl.semaphore_wait(barrier, greeters(1) + tp_size - 1)
    load_wait(qd.at[:, first], load_sem.at[0])
    send_pair(0)
    hop(0)

    @pl.when(jnp.logical_not(has_left))
    def _():
        spot = lax.broadcasted_iota(jnp.int32, left_stats.shape, 1)
        left_stats[...] = jnp.where((spot & 2) == 0, NEG_FILL, 0.0)
        keys = pl.ds(moved * LANES, width - moved * LANES)
        kv[:, first, keys] = jnp.zeros((2, rows, width - moved * LANES), BF16)

    load_wait(table_rows, load_sem.at[2])
    for h in range(heads):
        row = table_rows[pl.ds(col * heads + h, 1), :] * LOG2E
        build_bias(row, bias_ref, h // 2, h % 2)

    load_wait(kv.at[:, second], load_sem.at[1])

    low = lax.broadcasted_iota(jnp.int32, (BLK, LANES), 1) < HEAD_DIM
    scale = HEAD_DIM ** -0.5
    sums, tops = {}, {}

    def split(x):
        zero = jnp.zeros_like(x)
        return jnp.concatenate([jnp.where(low, x, zero), jnp.where(low, zero, x)], axis=0)

    def queries(p, mine):
        cols = pl.ds(p * LANES, LANES)
        return split(qd[0, mine, cols] * jnp.asarray(scale, BF16)), split(qd[1, mine, cols])

    def tile(p, half, halo):
        cols = pl.ds(p * LANES, LANES)
        mine = pl.ds(half * BLK + (rows if halo else 0), BLK)
        start, size, row = (
            (half * BLK, REACH - half * BLK, 0)
            if halo
            else (0, (half + 1) * BLK, REACH - half * BLK)
        )
        keys = pl.ds(rows + start, size)
        return kv[0, keys, cols], kv[1, keys, cols], *queries(p, mine), pl.ds(row, size)

    def put(stats, p, half, which, value):
        for lane in range(2):
            spot = pl.ds(half * 4 + which * 2 + lane, 1)
            stats[p, spot, :] = value[:, lane * BLK : (lane + 1) * BLK]

    def get(stats, p, half, which):
        spots = [pl.ds(half * 4 + which * 2 + lane, 1) for lane in range(2)]
        return jnp.concatenate([stats[p, spot, :] for spot in spots], axis=1)

    def partial_softmax(p, half, halo, stats):
        k_blk, v_blk, qq, dd, band = tile(p, half, halo)
        scores = dot(k_blk, qq, NT) * LOG2E + bias_ref[p, band]
        dprobs = dot(v_blk, dd, NT)
        peak = jnp.max(scores, axis=0, keepdims=True)
        grown = jnp.exp2(scores - peak)
        total = jnp.sum(grown, axis=0, keepdims=True)
        put(stats, p, half, 0, peak + jnp.log2(total))
        put(stats, p, half, 1, jnp.sum(grown * dprobs, axis=0, keepdims=True) / total)
        return grown, dprobs, peak

    def products(k_blk, qq, dd, probs, dscores):
        ds_half = dscores.astype(BF16)
        flat = dot(k_blk, ds_half, TN)
        both = jnp.concatenate([flat[:HEAD_DIM, :BLK], flat[HEAD_DIM:, BLK:]], axis=0)
        return (
            dot(ds_half, qq, NN),
            dot(probs.astype(BF16), dd, NN),
            jnp.transpose(both) * scale,
        )

    def tile_probs(p, half, grown, dprobs, peak, stats, others):
        n1, i1 = get(stats, p, half, 0), get(stats, p, half, 1)
        n2, i2 = get(others, p, half, 0), get(others, p, half, 1)
        top = jnp.maximum(n1, n2)
        a1, a2 = jnp.exp2(n1 - top), jnp.exp2(n2 - top)
        inverse = 1.0 / (a1 + a2)
        inner = (i1 * a1 + i2 * a2) * inverse
        probs = grown * (jnp.exp2(peak - top) * inverse)
        return probs, probs * (dprobs - inner)

    def tile_grads(p, half, halo, probs, dscores):
        k_blk, _, qq, dd, _ = tile(p, half, halo)
        return products(k_blk, qq, dd, probs, dscores)

    places = (pl.ds(0, BLK), pl.ds(BLK, 2 * BLK))
    for p in range(moved):
        for half in range(2):
            grown, dprobs, peak = partial_softmax(p, half, False, local_stats)
            grown_ref[p, places[half], :] = grown
            dprob_ref[p, places[half], :] = dprobs
            peak_ref[p, pl.ds(half, 1), :] = peak

    @pl.when(has_left)
    def _():
        local_copy().start()

    send_pair(1)

    def after_stats(p):
        send_pair(p + 2)
        if p == moved - 1:
            for rest in range(p + 3, pairs):
                send_pair(rest)

    def halo(p):
        @pl.when(has_right)
        def _():
            query_copy(p, 1).wait_recv()
            kept = [partial_softmax(p, half, True, halo_stats) for half in range(2)]
            halo_copy(p).start()
            after_stats(p)
            if p == 0:
                local_copy().wait_recv()
            (p0, s0), (p1, s1) = (
                tile_probs(p, half, *kept[half], halo_stats, right_stats) for half in range(2)
            )
            k0, v0, q0 = tile_grads(p, 0, True, p0, s0)
            k1, v1, q1 = tile_grads(p, 1, True, p1, s1)
            for ref, a, b in ((own_k, k0, k1), (own_v, v0, v1)):
                ref[p, :BLK, :] = a[:BLK]
                ref[p, BLK:, :] = a[BLK:] + b
            back_q[p, :BLK, :] = q0.astype(BF16)
            back_q[p, BLK:, :] = q1.astype(BF16)
            square_ref[p, :BLK, :] = s0[:BLK] + s1
            square_ref[p, BLK:REACH, :] = s0[BLK:]

        @pl.when(jnp.logical_not(has_right))
        def _():
            after_stats(p)
            own_k[p] = jnp.zeros((rows, LANES), F32)
            own_v[p] = jnp.zeros((rows, LANES), F32)
            square_ref[p, :REACH, :] = jnp.zeros((REACH, 2 * BLK), F32)

        hop(p + 1)

    def tally(p, square):
        for lane in range(2):
            sums[2 * p + lane], tops[2 * p + lane] = diagonals(
                square[:, lane * BLK : (lane + 1) * BLK]
            )

    def local(p, between=None):
        cols = pl.ds(p * LANES, LANES)

        @pl.when(has_left)
        def _():
            halo_copy(p).wait_recv()

        (p0, s0), (p1, s1) = (
            tile_probs(
                p, half,
                grown_ref[p, places[half], :], dprob_ref[p, places[half], :],
                peak_ref[p, pl.ds(half, 1), :],
                local_stats, left_stats,
            )
            for half in range(2)
        )
        square = jnp.concatenate(
            [
                square_ref[p, :BLK, :],
                square_ref[p, BLK:REACH, :] + s1[:BLK],
                s0 + s1[BLK:],
            ],
            axis=0,
        )
        tally(p, square)
        if between is not None:
            between()
        k0, v0, q0 = tile_grads(p, 0, False, p0, s0)
        k1, v1, q1 = tile_grads(p, 1, False, p1, s1)
        for out, ref, a, b in ((dk_ref, own_k, k0, k1), (dv_ref, own_v, v0, v1)):
            out[:BLK, cols] = (ref[p, :BLK, :] + a + b[:BLK]).astype(BF16)
            out[BLK:, cols] = (ref[p, BLK:, :] + b[BLK:]).astype(BF16)
        own_q[p, :BLK, :] = q0
        own_q[p, BLK:, :] = q1

    gate = jnp.where(has_left, 0.0, NEG_FILL)

    def full(p, between=None):
        cols = pl.ds(p * LANES, LANES)
        i = p - moved

        def half_probs(half):
            @pl.when(has_left)
            def _():
                key_copy(p, half).wait_recv()

            keys = pl.ds(half * BLK, BAND)
            qq, dd = queries(p, pl.ds(half * BLK, BLK))
            scores = dot(kv[0, keys, cols], qq, NT) * LOG2E + bias_ref[p]
            before = REACH - half * BLK
            scores = jnp.concatenate([scores[:before] + gate, scores[before:]], axis=0)
            dprobs = dot(kv[1, keys, cols], dd, NT)
            peak = jnp.max(scores, axis=0, keepdims=True)
            grown = jnp.exp2(scores - peak)
            inverse = 1.0 / jnp.sum(grown, axis=0, keepdims=True)
            inner = jnp.sum(grown * dprobs, axis=0, keepdims=True) * inverse
            probs = grown * inverse
            return probs, probs * (dprobs - inner)

        def half_grads(half, probs, dscores):
            qq, dd = queries(p, pl.ds(half * BLK, BLK))
            return products(kv[0, pl.ds(half * BLK, BAND), cols], qq, dd, probs, dscores)

        p1, s1 = half_probs(1)
        k1, v1, q1 = half_grads(1, p1, s1)
        p0, s0 = half_probs(0)
        tally(p, s0 + s1)
        if between is not None:
            between()
        k0, v0, q0 = half_grads(0, p0, s0)
        for which, ref, a, b in ((0, own_k, k0, k1), (1, own_v, v0, v1)):
            back_kv[i, which, :BLK, :] = a[:BLK].astype(BF16)
            back_kv[i, which, BLK:, :] = (a[BLK:REACH] + b[:BLK]).astype(BF16)
            ref[p, :BLK, :] = a[REACH:] + b[BLK:REACH]
            ref[p, BLK:, :] = b[REACH:]
        dq_ref[:BLK, cols] = q0.astype(BF16)
        dq_ref[BLK:, cols] = q1.astype(BF16)

    def piece_copy(k):
        target = lax.rem(me + k, sp_size)
        return remote(
            pieces.at[target * part // CLIP], piece_got.at[k - 1], 6, misc_recv.at[1], target
        )

    def all_pieces():
        return remote(piece_got, piece_got, 6, misc_recv.at[1], left)

    def share_copy(k):
        return pltpu.make_async_remote_copy(
            src_ref=shares.at[0],
            dst_ref=shares.at[k],
            send_sem=send_sem.at[7],
            recv_sem=misc_recv.at[2],
            device_id=(me, lax.rem(col + k, tp_size)),
            device_id_type=MESH,
        )

    def all_shares():
        rest = shares.at[pl.ds(1, tp_size - 1)]
        return remote(rest, rest, 7, misc_recv.at[2], left)

    def send_pieces():
        for r in range(moved + 1, rounds + 1):
            hop(r)
        y = jnp.concatenate([sums[h] for h in range(heads)], axis=0)
        beyond = jnp.sum(
            y[:, BLK : 2 * BLK] + jnp.concatenate([tops[h] for h in range(heads)], axis=0),
            axis=1, keepdims=True,
        )
        spot = lax.broadcasted_iota(jnp.int32, (heads, BLK), 1)
        pieces[0] = y[:, 2 * BLK :]
        pieces[1] = y[:, :BLK] + jnp.where(spot == BLK - 1, beyond, 0.0)
        for k in range(1, sp_size):
            piece_copy(k).start()
        for p in range(pairs - 1):
            send_back(p)

    for p in range(moved):
        halo(p)
        if p:
            local(p - 1)
    last = pairs - 1
    for p in range(moved, last):
        full(p)
        if p == moved:
            local(moved - 1)
    if moved < last:
        full(last, send_pieces)
    else:
        full(last, lambda: local(moved - 1, send_pieces))
    send_back(last)

    all_pieces().wait_recv()
    total = pieces[me * part // CLIP]
    for k in range(1, sp_size):
        total = total + piece_got[k - 1]
    shares[0] = pltpu.roll(total, lax.rem(CLIP - lax.rem(me * part, CLIP), CLIP), 1)
    for k in range(1, tp_size):
        share_copy(k).start()

    def finish(p):
        cols = pl.ds(p * LANES, LANES)
        if p < moved:
            @pl.when(has_left)
            def _():
                back_copy(p).wait_recv()
                dq_ref[:, cols] = (own_q[p] + got_q[p].astype(F32)).astype(BF16)

            @pl.when(jnp.logical_not(has_left))
            def _():
                dq_ref[:, cols] = own_q[p].astype(BF16)
        else:
            i = p - moved

            @pl.when(has_right)
            def _():
                key_back_copy(p).wait_recv()
                dk_ref[:, cols] = (own_k[p] + got_kv[i, 0].astype(F32)).astype(BF16)
                dv_ref[:, cols] = (own_v[p] + got_kv[i, 1].astype(F32)).astype(BF16)

            @pl.when(jnp.logical_not(has_right))
            def _():
                dk_ref[:, cols] = own_k[p].astype(BF16)
                dv_ref[:, cols] = own_v[p].astype(BF16)

    for p in range(pairs):
        finish(p)
    all_shares().wait_recv()
    stacked = jnp.concatenate(
        [shares[lax.rem(col + tp_size - t, tp_size)] for t in range(tp_size)], axis=0
    )
    dt_ref[...] = jnp.transpose(stacked)[:part]

    all_pieces().wait_send()
    all_shares().wait_send()

    @pl.when(has_left)
    def _():
        query_copy(0, moved).wait_send()
        local_copy().wait_send()
        remote(back_kv, got_kv, 5, misc_recv.at[0], left).wait_send()

    @pl.when(has_right)
    def _():
        all_keys().wait_send()
        remote(halo_stats, left_stats, 3, misc_recv.at[0], right).wait_send()
        remote(back_q, got_q, 4, misc_recv.at[0], right).wait_send()


def shards(sp_size, tp_size, query_rows, key_rows, value_rows, out_grad, rel_bias):
    rows, width = query_rows.shape
    pairs = width // LANES
    heads = width // HEAD_DIM
    part = 2 * CLIP // sp_size
    moved = pairs - 1
    rounds = max(sp_size - 2, 0).bit_length()
    assert rows == REACH and REACH == 2 * BLK and CLIP == BLK
    like = jax.ShapeDtypeStruct((rows, width), BF16)
    dma = pltpu.SemaphoreType.DMA
    shapes = (like, like, like, jax.ShapeDtypeStruct((part, heads * tp_size), F32))
    results = pl.pallas_call(
        partial(kernel, sp_size, tp_size, moved),
        out_shape=shapes,
        in_specs=[pl.BlockSpec(memory_space=pltpu.HBM)] * 5,
        out_specs=tuple([pl.BlockSpec(memory_space=pltpu.VMEM)] * 4),
        scratch_shapes=[
            pltpu.VMEM((2, 2 * rows, width), BF16),
            pltpu.VMEM((2, 2 * rows, width), BF16),
            pltpu.VMEM((pairs, BAND, 2 * BLK), F32),
            pltpu.VMEM((moved, REACH, 2 * BLK), F32),
            pltpu.VMEM((moved, BAND, 2 * BLK), F32),
            pltpu.VMEM((moved, BAND, 2 * BLK), F32),
            pltpu.VMEM((moved, 8, 2 * BLK), F32),
            pltpu.VMEM((pairs, rows, LANES), F32),
            pltpu.VMEM((pairs, rows, LANES), F32),
            pltpu.VMEM((moved, rows, LANES), F32),
            pltpu.VMEM((moved, rows, LANES), BF16),
            pltpu.VMEM((moved, rows, LANES), BF16),
            pltpu.VMEM((pairs - moved, 2, rows, LANES), BF16),
            pltpu.VMEM((pairs - moved, 2, rows, LANES), BF16),
            pltpu.VMEM((moved, 8, BLK), F32),
            pltpu.VMEM((moved, 8, BLK), F32),
            pltpu.VMEM((moved, 8, BLK), F32),
            pltpu.VMEM((moved, 8, BLK), F32),
            pltpu.VMEM(rel_bias.shape[::-1], F32),
            pltpu.VMEM((2, heads, BLK), F32),
            pltpu.VMEM((sp_size - 1, heads, BLK), F32),
            pltpu.VMEM((tp_size, heads, BLK), F32),
            dma((3,)),
            pltpu.SemaphoreType.REGULAR((rounds,)),
            dma((8,)),
            dma((2 * pairs - moved,)),
            dma((pairs,)),
            dma((moved,)),
            dma((3,)),
        ],
        compiler_params=pltpu.CompilerParams(
            collective_id=0, has_side_effects=True, vmem_limit_bytes=48 * 1024 * 1024
        ),
    )(*[pltpu.with_memory_space_constraint(x, pltpu.HBM) for x in (query_rows, key_rows, value_rows, out_grad, jnp.transpose(rel_bias))])
    return pl.pallas_call(
        write_out,
        out_shape=shapes,
        in_specs=[pl.BlockSpec(memory_space=pl.ANY)] * 4,
        out_specs=tuple([pl.BlockSpec(memory_space=pltpu.HBM)] * 4),
        scratch_shapes=[dma((4,))],
        compiler_params=pltpu.CompilerParams(vmem_limit_bytes=1024 * 1024),
    )(*results)


def write_out(*refs):
    sem = refs[-1]
    copies = [pltpu.make_async_copy(refs[i], refs[4 + i], sem.at[i]) for i in range(4)]
    for copy in copies:
        copy.start()
    for copy in copies:
        copy.wait()


def solution(mesh):
    return jax.shard_map(
        partial(shards, mesh.shape["sp"], mesh.shape["tp"]),
        mesh=mesh,
        in_specs=(P("sp", "tp"), P("sp", "tp"), P("sp", "tp"), P("sp", "tp"), P()),
        out_specs=(P("sp", "tp"), P("sp", "tp"), P("sp", "tp"), P("sp", None)),
        check_vma=False,
    )
```

time: 32.1 us -> 29.8 us (0.928)
  Pallas kernels: 31.3 us -> 29 us
    pallas_call x1, Pallas kernels: 30.3 us -> 28.1 us  [shards(): pl.pallas_call(partial(kernel, sp_size, tp_size, moved), out_shape=shapes...]
where the time goes in v1:
time: 29.8 us; the launch traced here: 29.7 us
  Pallas kernels  29 us (97%)
  between operations  0.64 us (2%)
    pallas_call x1, Pallas kernels, shards(): pl.pallas_call(partial(kernel, sp_size, tp_size, moved), out_shape=shapes...  28.1 us
    pallas_call x1, Pallas kernels, shards(): pl.pallas_call(write_out, out_shape=shapes, in_specs=[pl.BlockSpec(memory...  0.91 us

profile of v1, /device:TPU:0, one launch (start us, length us, event | category | flops | bytes accessed | tf_op | source)
XLA Modules:
  0.0 29.7 jit_solution(8509917383979044262)
XLA Ops:
  0.6 28.1 %shard_map.84 = (bf16[256,512]{1,0:T(8,128)(2,1)S(1)}, bf16[256,512]{1,0:T(8,128)(2,1)S(1)}, bf16[256,512]{1,0:T(8,128)(2,1)S(1)}, f32[32,32]{1,0:T(8,128)S(1)}) custom-call(bf16[256,512]{1,0:T(8,128)(2,1)} %q_hbm.1, bf16[256,512]{1,0:T(8,128)(2,1)} %k_hbm.1, bf16[256,512]{1,0:T(8,128)(2,1)} %v_hbm.1, bf16[256,512]{1,0:T(8,128)(2,1)} %d_hbm.1, f32[32,256]{1,0:T(8,128)} %bitcast.1), custom_call_target="tpu_custom_call" | custom-call | tf_op jit(solution)/shard_map/pallas_call | solution.py:551
  28.7 0.9 %shard_map.85 = (bf16[256,512]{1,0:T(8,128)(2,1)}, bf16[256,512]{1,0:T(8,128)(2,1)}, bf16[256,512]{1,0:T(8,128)(2,1)}, f32[32,32]{1,0:T(8,128)}) custom-call(bf16[256,512]{1,0:T(8,128)(2,1)S(1)} %get-tuple-element.8.refs_0_, bf16[256,512]{1,0:T(8,128)(2,1)S(1)} %get-tuple-element.9.refs_1_, bf16[256,512]{1,0:T(8,128)(2,1)S(1)} %get-tuple-element.10.refs_2_, ...), custom_call_target="tpu_custom_call" | custom-call | tf_op jit(solution)/shard_map/pallas_call | solution.py:591

commit v2 on v1

--- a/solution.py
+++ b/solution.py
@@ -38,60 +38,64 @@
     return pltpu.roll(x, amount, 1) if amount else x
 
 
-def row_turned(x, sign):
-    row = lax.broadcasted_iota(jnp.int32, x.shape, 0)
-    for bit in (1, 2, 4):
-        x = jnp.where((row & bit) != 0, turned(x, sign * bit), x)
-    return x
+def grid(axis):
+    return lax.broadcasted_iota(jnp.int32, (BLK, BLK), axis)
 
 
 def build_bias(table_row, bias_ref, pair, lane):
-    last = table_row[:, 2 * CLIP - 1 :]
-    flat = jnp.broadcast_to(last, (1, BLK))
-    shape = (8, BLK)
-    line = jnp.concatenate([table_row[:, CLIP:], flat, table_row[:, :CLIP]], axis=1)
-    base = row_turned(jnp.broadcast_to(line, (8, WRAP)), 1)
-    query = lax.broadcasted_iota(jnp.int32, shape, 1)
+    def shear(half):
+        return pltpu.roll(
+            jnp.broadcast_to(half, (BLK, BLK)), 0, 1, stride=1, stride_axis=0
+        )
+
+    ahead, behind = shear(table_row[:, CLIP:]), shear(table_row[:, :CLIP])
+    flat = jnp.broadcast_to(table_row[:, 2 * CLIP - 1 :], (BLK, BLK))
+    key, query = grid(0), grid(1)
+    later = query >= key
     cols = pl.ds(lane * BLK, BLK)
-    flat8 = jnp.broadcast_to(last, shape)
-    for group in range(BAND // 8):
-        row = group * 8
-        if row < BLK:
-            tile = flat8
-        else:
-            sheared = turned(base, row % BLK)
-            tile = sheared[:, BLK : 2 * BLK] if row < 2 * BLK else sheared[:, :BLK]
-        if row < SEG:
-            tile = jnp.where(query >= SEG, NEG_FILL, tile)
-        if row >= BAND - SEG:
-            tile = jnp.where(query < SEG, NEG_FILL, tile)
-        bias_ref[pair, pl.ds(row, 8), cols] = tile
+    bias_ref[pair, :BLK, cols] = jnp.where((key < SEG) & (query >= SEG), NEG_FILL, flat)
+    bias_ref[pair, BLK : 2 * BLK, cols] = jnp.where(later, flat, ahead)
+    bias_ref[pair, 2 * BLK :, cols] = jnp.where(
+        (key >= SEG) & (query < SEG), NEG_FILL, jnp.where(later, ahead, behind)
+    )
+
+
+def unshear(square):
+    parts = [turned(square[8 * g : 8 * g + 8], -8 * g) for g in range(BLK // 8)]
+    while len(parts) > 1:
+        parts = [a + b for a, b in zip(parts[::2], parts[1::2])]
+    row = lax.broadcasted_iota(jnp.int32, (8, BLK), 0)
+    result = parts[0]
+    for i in range(1, 8):
+        result = jnp.where(row == i, turned(parts[0], -i), result)
+    return jnp.sum(result, axis=0, keepdims=True)
 
 
 def diagonals(square):
-    parts = []
-    for group in range(BLK // 8):
-        near = square[2 * BLK + group * 8 : 2 * BLK + group * 8 + 8]
-        far = square[BLK + group * 8 : BLK + group * 8 + 8]
-        parts.append(jnp.concatenate([near, far, jnp.zeros_like(near)], axis=1))
-    step = 8
-    while len(parts) > 1:
-        parts = [a + turned(b, -step) for a, b in zip(parts[::2], parts[1::2])]
-        step *= 2
-    sums = jnp.sum(row_turned(parts[0], -1), axis=0, keepdims=True)
-    return sums, jnp.sum(square[:BLK], axis=0, keepdims=True)
+    top, far, near = square[:BLK], square[BLK : 2 * BLK], square[2 * BLK :]
+    later = grid(1) >= grid(0)
+    beyond = jnp.sum(top + jnp.where(later, far, 0.0), axis=0, keepdims=True)
+    return (
+        unshear(jnp.where(later, 0.0, near)),
+        unshear(jnp.where(later, near, far)),
+        beyond,
+    )
 
 
 def kernel(
-    sp_size, tp_size, moved,
+    sp_size, tp_size, moved, direct,
     q_hbm, k_hbm, v_hbm, d_hbm, table_hbm,
     dq_ref, dk_ref, dv_ref, dt_ref,
-    qd, kv, bias_ref, square_ref, grown_ref, dprob_ref, peak_ref,
+    qd, got_qd, kv, bias_ref, square_ref, grown_ref, dprob_ref, peak_ref,
     own_k, own_v, own_q, back_q, got_q, back_kv, got_kv,
     local_stats, right_stats, halo_stats, left_stats,
-    table_rows, pieces, piece_got, shares,
+    table_rows, pieces, exchange_a, exchange_b, exchange_c, exchange_d,
     load_sem, hop_sem, send_sem, seq_recv, back_recv, halo_recv, misc_recv,
 ):
+    if direct:
+        packs, pack_got, turns, stack = exchange_a, exchange_b, exchange_c, exchange_d
+    else:
+        piece_got, shares = exchange_a, exchange_b
     rows, width = q_hbm.shape
     pairs = width // LANES
     heads = width // HEAD_DIM
@@ -102,13 +106,18 @@
     has_right = me < sp_size - 1
     left = jnp.maximum(me - 1, 0)
     right = jnp.minimum(me + 1, sp_size - 1)
-    first, second = pl.ds(0, rows), pl.ds(rows, rows)
-
-    pltpu.make_async_copy(q_hbm, qd.at[0, first], load_sem.at[0]).start()
-    pltpu.make_async_copy(d_hbm, qd.at[1, first], load_sem.at[0]).start()
-    pltpu.make_async_copy(table_hbm, table_rows, load_sem.at[2]).start()
-    pltpu.make_async_copy(k_hbm, kv.at[0, second], load_sem.at[1]).start()
-    pltpu.make_async_copy(v_hbm, kv.at[1, second], load_sem.at[1]).start()
+    prev, own = pl.ds(0, rows), pl.ds(rows, rows)
+
+    def columns(p):
+        return pl.ds(p * LANES, LANES)
+
+    for p in range(pairs):
+        for i, src in enumerate((q_hbm, d_hbm)):
+            pltpu.make_async_copy(src.at[:, columns(p)], qd.at[p, i], load_sem.at[2 + p]).start()
+    pltpu.make_async_copy(table_hbm, table_rows, load_sem.at[0]).start()
+    for p in range(pairs):
+        for i, src in enumerate((k_hbm, v_hbm)):
+            pltpu.make_async_copy(src.at[:, columns(p)], kv.at[p, i, own], load_sem.at[1]).start()
 
     barrier = pltpu.get_barrier_semaphore()
 
@@ -130,7 +139,7 @@
             barrier, inc=1, device_id=(me, lax.rem(col + k, tp_size)), device_id_type=MESH
         )
 
-    rounds = hop_sem.shape[0]
+    rounds = hop_sem.shape[0] - 1
 
     def hop(r):
         if 0 < r <= rounds:
@@ -148,25 +157,24 @@
             device_id_type=MESH,
         )
 
-    def query_copy(start, count):
-        cols = pl.ds(start * LANES, count * LANES)
+    def query_copy(p):
+        return remote(qd.at[p], got_qd.at[p], 0, seq_recv.at[p], left)
+
+    def all_queries():
+        return remote(qd.at[pl.ds(0, moved)], got_qd, 0, misc_recv.at[0], left)
+
+    def key_copy(p, block):
         return remote(
-            qd.at[:, first, cols], qd.at[:, second, cols], 0, seq_recv.at[start], left
-        )
-
-    def key_copy(p, block):
-        cols = pl.ds(p * LANES, LANES)
-        return remote(
-            kv.at[:, pl.ds(rows + block * BLK, BLK), cols],
-            kv.at[:, pl.ds(block * BLK, BLK), cols],
+            kv.at[p, :, pl.ds(rows + block * BLK, BLK)],
+            kv.at[p, :, pl.ds(block * BLK, BLK)],
             1,
             seq_recv.at[p + block * (pairs - moved)],
             right,
         )
 
     def all_keys():
-        cols = pl.ds(moved * LANES, width - moved * LANES)
-        return remote(kv.at[:, second, cols], kv.at[:, first, cols], 1, misc_recv.at[0], right)
+        keyed = pl.ds(moved, pairs - moved)
+        return remote(kv.at[keyed, :, own], kv.at[keyed, :, prev], 1, misc_recv.at[0], right)
 
     def local_copy():
         return remote(local_stats, right_stats, 2, misc_recv.at[0], left)
@@ -181,16 +189,10 @@
         i = p - moved
         return remote(back_kv.at[i], got_kv.at[i], 5, back_recv.at[p], left)
 
-    def send_pair(p):
-        if p < moved:
-            @pl.when(has_left)
-            def _():
-                query_copy(p, 1).start()
-        elif p < pairs:
-            @pl.when(has_right)
-            def _():
-                for block in (1, 0):
-                    key_copy(p, block).start()
+    def send_queries(p):
+        @pl.when(has_left)
+        def _():
+            query_copy(p).start()
 
     def send_back(p):
         if p < moved:
@@ -206,46 +208,46 @@
         pltpu.make_async_copy(refs, refs, sem).wait()
 
     pl.semaphore_wait(barrier, greeters(1) + tp_size - 1)
-    load_wait(qd.at[:, first], load_sem.at[0])
-    send_pair(0)
+    load_wait(qd.at[0], load_sem.at[2])
+    send_queries(0)
     hop(0)
 
     @pl.when(jnp.logical_not(has_left))
     def _():
         spot = lax.broadcasted_iota(jnp.int32, left_stats.shape, 1)
         left_stats[...] = jnp.where((spot & 2) == 0, NEG_FILL, 0.0)
-        keys = pl.ds(moved * LANES, width - moved * LANES)
-        kv[:, first, keys] = jnp.zeros((2, rows, width - moved * LANES), BF16)
-
-    load_wait(table_rows, load_sem.at[2])
+        kv[moved:, :, prev] = jnp.zeros((pairs - moved, 2, rows, LANES), BF16)
+
+    load_wait(table_rows, load_sem.at[0])
     for h in range(heads):
         row = table_rows[pl.ds(col * heads + h, 1), :] * LOG2E
         build_bias(row, bias_ref, h // 2, h % 2)
 
-    load_wait(kv.at[:, second], load_sem.at[1])
+    for p in range(1, pairs):
+        load_wait(qd.at[p], load_sem.at[2 + p])
+    load_wait(kv.at[:, :, own], load_sem.at[1])
 
     low = lax.broadcasted_iota(jnp.int32, (BLK, LANES), 1) < HEAD_DIM
     scale = HEAD_DIM ** -0.5
-    sums, tops = {}, {}
+    sums = {}
 
     def split(x):
         zero = jnp.zeros_like(x)
         return jnp.concatenate([jnp.where(low, x, zero), jnp.where(low, zero, x)], axis=0)
 
-    def queries(p, mine):
-        cols = pl.ds(p * LANES, LANES)
-        return split(qd[0, mine, cols] * jnp.asarray(scale, BF16)), split(qd[1, mine, cols])
+    def queries(ref, p, half):
+        mine = pl.ds(half * BLK, BLK)
+        return split(ref[p, 0, mine] * jnp.asarray(scale, BF16)), split(ref[p, 1, mine])
 
     def tile(p, half, halo):
-        cols = pl.ds(p * LANES, LANES)
-        mine = pl.ds(half * BLK + (rows if halo else 0), BLK)
         start, size, row = (
             (half * BLK, REACH - half * BLK, 0)
             if halo
             else (0, (half + 1) * BLK, REACH - half * BLK)
         )
         keys = pl.ds(rows + start, size)
-        return kv[0, keys, cols], kv[1, keys, cols], *queries(p, mine), pl.ds(row, size)
+        ref = got_qd if halo else qd
+        return kv[p, 0, keys], kv[p, 1, keys], *queries(ref, p, half), pl.ds(row, size)
 
     def put(stats, p, half, which, value):
         for lane in range(2):
@@ -303,18 +305,47 @@
     def _():
         local_copy().start()
 
-    send_pair(1)
+    if moved > 1:
+        send_queries(1)
+
+    even = lax.rem(me, 2) == 0
+    core = lax.rem(col, 2)
+    early = has_right & (even | (core == 0))
+    keyed = [(p, block) for p in range(moved, pairs) for block in (1, 0)]
+    turn = moved - 2 if moved > 1 else 0
+
+    def send_keys():
+        for p, block in keyed:
+            key_copy(p, block).start()
 
     def after_stats(p):
-        send_pair(p + 2)
+        if p + 2 < moved:
+            send_queries(p + 2)
+        if p == turn:
+            @pl.when(has_right & jnp.logical_not(even) & (core == 0))
+            def _():
+                pl.semaphore_signal(
+                    hop_sem.at[rounds], inc=1, device_id=(me, col + 1), device_id_type=MESH
+                )
+
+            @pl.when(early)
+            def _():
+                send_keys()
+
         if p == moved - 1:
-            for rest in range(p + 3, pairs):
-                send_pair(rest)
+            for done in range(p):
+                send_back(done)
+
+    def late_keys():
+        @pl.when(has_right & jnp.logical_not(early))
+        def _():
+            pl.semaphore_wait(hop_sem.at[rounds], 1)
+            send_keys()
 
     def halo(p):
         @pl.when(has_right)
         def _():
-            query_copy(p, 1).wait_recv()
+            query_copy(p).wait_recv()
             kept = [partial_softmax(p, half, True, halo_stats) for half in range(2)]
             halo_copy(p).start()
             after_stats(p)
@@ -344,11 +375,9 @@
 
     def tally(p, square):
         for lane in range(2):
-            sums[2 * p + lane], tops[2 * p + lane] = diagonals(
-                square[:, lane * BLK : (lane + 1) * BLK]
-            )
-
-    def local(p, between=None):
+            sums[2 * p + lane] = diagonals(square[:, lane * BLK : (lane + 1) * BLK])
+
+    def local(p):
         cols = pl.ds(p * LANES, LANES)
 
         @pl.when(has_left)
@@ -373,8 +402,6 @@
             axis=0,
         )
         tally(p, square)
-        if between is not None:
-            between()
         k0, v0, q0 = tile_grads(p, 0, False, p0, s0)
         k1, v1, q1 = tile_grads(p, 1, False, p1, s1)
         for out, ref, a, b in ((dk_ref, own_k, k0, k1), (dv_ref, own_v, v0, v1)):
@@ -385,7 +412,7 @@
 
     gate = jnp.where(has_left, 0.0, NEG_FILL)
 
-    def full(p, between=None):
+    def full(p, before=None, between=None):
         cols = pl.ds(p * LANES, LANES)
         i = p - moved
 
@@ -395,11 +422,11 @@
                 key_copy(p, half).wait_recv()
 
             keys = pl.ds(half * BLK, BAND)
-            qq, dd = queries(p, pl.ds(half * BLK, BLK))
-            scores = dot(kv[0, keys, cols], qq, NT) * LOG2E + bias_ref[p]
+            qq, dd = queries(qd, p, half)
+            scores = dot(kv[p, 0, keys], qq, NT) * LOG2E + bias_ref[p]
             before = REACH - half * BLK
             scores = jnp.concatenate([scores[:before] + gate, scores[before:]], axis=0)
-            dprobs = dot(kv[1, keys, cols], dd, NT)
+            dprobs = dot(kv[p, 1, keys], dd, NT)
             peak = jnp.max(scores, axis=0, keepdims=True)
             grown = jnp.exp2(scores - peak)
             inverse = 1.0 / jnp.sum(grown, axis=0, keepdims=True)
@@ -408,12 +435,16 @@
             return probs, probs * (dprobs - inner)
 
         def half_grads(half, probs, dscores):
-            qq, dd = queries(p, pl.ds(half * BLK, BLK))
-            return products(kv[0, pl.ds(half * BLK, BAND), cols], qq, dd, probs, dscores)
+            qq, dd = queries(qd, p, half)
+            return products(kv[p, 0, pl.ds(half * BLK, BAND)], qq, dd, probs, dscores)
 
         p1, s1 = half_probs(1)
         k1, v1, q1 = half_grads(1, p1, s1)
+        if before is not None:
+            before()
         p0, s0 = half_probs(0)
+        if p == pairs - 1:
+            send_back(moved - 1)
         tally(p, s0 + s1)
         if between is not None:
             between()
@@ -426,14 +457,24 @@
         dq_ref[:BLK, cols] = q0.astype(BF16)
         dq_ref[BLK:, cols] = q1.astype(BF16)
 
-    def piece_copy(k):
+    def piece_copy(k, t):
         target = lax.rem(me + k, sp_size)
-        return remote(
-            pieces.at[target * part // CLIP], piece_got.at[k - 1], 6, misc_recv.at[1], target
+        if direct:
+            src, dst = packs.at[target], pack_got.at[col * sp_size + me]
+        else:
+            src, dst = pieces.at[target * part // CLIP], piece_got.at[k - 1]
+        return pltpu.make_async_remote_copy(
+            src_ref=src,
+            dst_ref=dst,
+            send_sem=send_sem.at[6],
+            recv_sem=misc_recv.at[1],
+            device_id=(target, lax.rem(col + t, tp_size)),
+            device_id_type=MESH,
         )
 
     def all_pieces():
-        return remote(piece_got, piece_got, 6, misc_recv.at[1], left)
+        ref = pack_got.at[pl.ds(1, sp_size * tp_size - 1)] if direct else piece_got
+        return remote(ref, ref, 6, misc_recv.at[1], left)
 
     def share_copy(k):
         return pltpu.make_async_remote_copy(
@@ -449,44 +490,69 @@
         rest = shares.at[pl.ds(1, tp_size - 1)]
         return remote(rest, rest, 7, misc_recv.at[2], left)
 
+    groups = CLIP // part
+    folded = exchange_a.shape[1]
+    wide = heads // folded
+
+    def fold():
+        block = lax.broadcasted_iota(jnp.int32, (folded, CLIP), 1) // part
+        for side in range(2):
+            for a in range(groups):
+                turns[a] = turned(pieces[side], part * a)
+            for m in range(groups):
+                pack = jnp.zeros((folded, CLIP), F32)
+                for j in range(wide):
+                    line = turns[(j - m) % groups, pl.ds(j, folded, stride=wide), :]
+                    pack = jnp.where(block == j, line, pack)
+                packs[side * groups + m] = pack
+
+    def unfold():
+        total = []
+        for t in range(tp_size):
+            line = pack_got[t * sp_size]
+            for k in range(1, sp_size):
+                line = line + pack_got[t * sp_size + k]
+            total.append(line)
+        total = jnp.concatenate(total, axis=0)
+        for j in range(wide):
+            stack[pl.ds(j, folded * tp_size, stride=wide), :] = turned(total, -part * j)
+        dt_ref[...] = jnp.transpose(stack[...])[:part]
+
     def send_pieces():
         for r in range(moved + 1, rounds + 1):
             hop(r)
-        y = jnp.concatenate([sums[h] for h in range(heads)], axis=0)
-        beyond = jnp.sum(
-            y[:, BLK : 2 * BLK] + jnp.concatenate([tops[h] for h in range(heads)], axis=0),
-            axis=1, keepdims=True,
-        )
+        behind, ahead, beyond = (
+            jnp.concatenate([sums[h][i] for h in range(heads)], axis=0) for i in range(3)
+        )
+        beyond = jnp.sum(beyond, axis=1, keepdims=True)
         spot = lax.broadcasted_iota(jnp.int32, (heads, BLK), 1)
-        pieces[0] = y[:, 2 * BLK :]
-        pieces[1] = y[:, :BLK] + jnp.where(spot == BLK - 1, beyond, 0.0)
-        for k in range(1, sp_size):
-            piece_copy(k).start()
-        for p in range(pairs - 1):
-            send_back(p)
+        pieces[0] = behind
+        pieces[1] = ahead + jnp.where(spot == BLK - 1, beyond, 0.0)
+        if direct:
+            fold()
+            pack_got[col * sp_size + me] = packs[me]
+        for k in range(sp_size):
+            for t in range(tp_size if direct else 1):
+                if k or t:
+                    piece_copy(k, t).start()
 
     for p in range(moved):
         halo(p)
         if p:
             local(p - 1)
+        if p == turn:
+            late_keys()
     last = pairs - 1
     for p in range(moved, last):
         full(p)
+        send_back(p)
         if p == moved:
             local(moved - 1)
     if moved < last:
-        full(last, send_pieces)
+        full(last, None, send_pieces)
     else:
-        full(last, lambda: local(moved - 1, send_pieces))
+        full(last, lambda: local(moved - 1), send_pieces)
     send_back(last)
-
-    all_pieces().wait_recv()
-    total = pieces[me * part // CLIP]
-    for k in range(1, sp_size):
-        total = total + piece_got[k - 1]
-    shares[0] = pltpu.roll(total, lax.rem(CLIP - lax.rem(me * part, CLIP), CLIP), 1)
-    for k in range(1, tp_size):
-        share_copy(k).start()
 
     def finish(p):
         cols = pl.ds(p * LANES, LANES)
@@ -513,20 +579,33 @@
                 dk_ref[:, cols] = own_k[p].astype(BF16)
                 dv_ref[:, cols] = own_v[p].astype(BF16)
 
-    for p in range(pairs):
+    for p in range(moved - 1):
         finish(p)
-    all_shares().wait_recv()
-    stacked = jnp.concatenate(
-        [shares[lax.rem(col + tp_size - t, tp_size)] for t in range(tp_size)], axis=0
-    )
-    dt_ref[...] = jnp.transpose(stacked)[:part]
+    all_pieces().wait_recv()
+    if direct:
+        unfold()
+    else:
+        total = pieces[me * part // CLIP]
+        for k in range(1, sp_size):
+            total = total + piece_got[k - 1]
+        shares[0] = pltpu.roll(total, lax.rem(CLIP - lax.rem(me * part, CLIP), CLIP), 1)
+        for k in range(1, tp_size):
+            share_copy(k).start()
+    for p in range(moved - 1, pairs):
+        finish(p)
+    if not direct:
+        all_shares().wait_recv()
+        stacked = jnp.concatenate(
+            [shares[lax.rem(col + tp_size - t, tp_size)] for t in range(tp_size)], axis=0
+        )
+        dt_ref[...] = jnp.transpose(stacked)[:part]
+        all_shares().wait_send()
 
     all_pieces().wait_send()
-    all_shares().wait_send()
 
     @pl.when(has_left)
     def _():
-        query_copy(0, moved).wait_send()
+        all_queries().wait_send()
         local_copy().wait_send()
         remote(back_kv, got_kv, 5, misc_recv.at[0], left).wait_send()
 
@@ -543,19 +622,35 @@
     heads = width // HEAD_DIM
     part = 2 * CLIP // sp_size
     moved = pairs - 1
-    rounds = max(sp_size - 2, 0).bit_length()
+    rounds = (sp_size - 1).bit_length()
+    direct = sp_size * tp_size <= 64 and part <= CLIP and heads % (CLIP // part) == 0
+    folded = heads * part // CLIP
+    exchange = [
+        pltpu.VMEM(shape, F32)
+        for shape in (
+            (
+                (sp_size, folded, CLIP),
+                (sp_size * tp_size, folded, CLIP),
+                (CLIP // part, heads, CLIP),
+                (tp_size * heads, CLIP),
+            )
+            if direct
+            else ((sp_size - 1, heads, CLIP), (tp_size, heads, CLIP), (8, CLIP), (8, CLIP))
+        )
+    ]
     assert rows == REACH and REACH == 2 * BLK and CLIP == BLK
     like = jax.ShapeDtypeStruct((rows, width), BF16)
     dma = pltpu.SemaphoreType.DMA
     shapes = (like, like, like, jax.ShapeDtypeStruct((part, heads * tp_size), F32))
     results = pl.pallas_call(
-        partial(kernel, sp_size, tp_size, moved),
+        partial(kernel, sp_size, tp_size, moved, direct),
         out_shape=shapes,
         in_specs=[pl.BlockSpec(memory_space=pltpu.HBM)] * 5,
         out_specs=tuple([pl.BlockSpec(memory_space=pltpu.VMEM)] * 4),
         scratch_shapes=[
-            pltpu.VMEM((2, 2 * rows, width), BF16),
-            pltpu.VMEM((2, 2 * rows, width), BF16),
+            pltpu.VMEM((pairs, 2, rows, LANES), BF16),
+            pltpu.VMEM((moved, 2, rows, LANES), BF16),
+            pltpu.VMEM((pairs, 2, 2 * rows, LANES), BF16),
             pltpu.VMEM((pairs, BAND, 2 * BLK), F32),
             pltpu.VMEM((moved, REACH, 2 * BLK), F32),
             pltpu.VMEM((moved, BAND, 2 * BLK), F32),
@@ -574,10 +669,9 @@
             pltpu.VMEM((moved, 8, BLK), F32),
             pltpu.VMEM(rel_bias.shape[::-1], F32),
             pltpu.VMEM((2, heads, BLK), F32),
-            pltpu.VMEM((sp_size - 1, heads, BLK), F32),
-            pltpu.VMEM((tp_size, heads, BLK), F32),
-            dma((3,)),
-            pltpu.SemaphoreType.REGULAR((rounds,)),
+            *exchange,
+            dma((2 + pairs,)),
+            pltpu.SemaphoreType.REGULAR((rounds + 1,)),
             dma((8,)),
             dma((2 * pairs - moved,)),
             dma((pairs,)),

time: 29.8 us -> 27.9 us (0.936)
  Pallas kernels: 29 us -> 27.1 us
    pallas_call x1, Pallas kernels: 28.1 us -> 26.2 us  [shards(): pl.pallas_call(partial(kernel, sp_size, tp_size, moved, direct), out_shap...]
where the time goes in v2:
time: 27.9 us; the launch traced here: 27.7 us
  Pallas kernels  27.1 us (97%)
  between operations  0.64 us (2%)
    pallas_call x1, Pallas kernels, shards(): pl.pallas_call(partial(kernel, sp_size, tp_size, moved, direct), out_shap...  26.2 us
    pallas_call x1, Pallas kernels, shards(): pl.pallas_call(write_out, out_shape=shapes, in_specs=[pl.BlockSpec(memory...  0.91 us

profile of v2, /device:TPU:0, one launch (start us, length us, event | category | flops | bytes accessed | tf_op | source)
XLA Modules:
  0.0 27.7 jit_solution(7771657524940524592)
XLA Ops:
  0.6 26.2 %shard_map.84 = (bf16[256,512]{1,0:T(8,128)(2,1)S(1)}, bf16[256,512]{1,0:T(8,128)(2,1)S(1)}, bf16[256,512]{1,0:T(8,128)(2,1)S(1)}, f32[32,32]{1,0:T(8,128)S(1)}) custom-call(bf16[256,512]{1,0:T(8,128)(2,1)} %q_hbm.1, bf16[256,512]{1,0:T(8,128)(2,1)} %k_hbm.1, bf16[256,512]{1,0:T(8,128)(2,1)} %v_hbm.1, bf16[256,512]{1,0:T(8,128)(2,1)} %d_hbm.1, f32[32,256]{1,0:T(8,128)} %bitcast.1), custom_call_target="tpu_custom_call" | custom-call | tf_op jit(solution)/shard_map/pallas_call | solution.py:645
  26.8 0.9 %shard_map.85 = (bf16[256,512]{1,0:T(8,128)(2,1)}, bf16[256,512]{1,0:T(8,128)(2,1)}, bf16[256,512]{1,0:T(8,128)(2,1)}, f32[32,32]{1,0:T(8,128)}) custom-call(bf16[256,512]{1,0:T(8,128)(2,1)S(1)} %get-tuple-element.8.refs_0_, bf16[256,512]{1,0:T(8,128)(2,1)S(1)} %get-tuple-element.9.refs_1_, bf16[256,512]{1,0:T(8,128)(2,1)S(1)} %get-tuple-element.10.refs_2_, ...), custom_call_target="tpu_custom_call" | custom-call | tf_op jit(solution)/shard_map/pallas_call | solution.py:685

commit v3 on v2

--- a/solution.py
+++ b/solution.py
@@ -21,6 +21,7 @@
 NEG_FILL = -1e30
 LOG2E = math.log2(math.e)
 MESH = pl.DeviceIdType.MESH
+LEFTWARD, RIGHTWARD = 0, 1
 F32 = jnp.float32
 BF16 = jnp.bfloat16
 
@@ -60,25 +61,28 @@
     )
 
 
-def unshear(square):
+def unshear(square, shift):
     parts = [turned(square[8 * g : 8 * g + 8], -8 * g) for g in range(BLK // 8)]
     while len(parts) > 1:
         parts = [a + b for a, b in zip(parts[::2], parts[1::2])]
     row = lax.broadcasted_iota(jnp.int32, (8, BLK), 0)
-    result = parts[0]
+    result = turned(parts[0], shift)
     for i in range(1, 8):
-        result = jnp.where(row == i, turned(parts[0], -i), result)
+        result = jnp.where(row == i, turned(parts[0], shift - i), result)
     return jnp.sum(result, axis=0, keepdims=True)
 
 
-def diagonals(square):
+def diagonals(square, shift):
     top, far, near = square[:BLK], square[BLK : 2 * BLK], square[2 * BLK :]
     later = grid(1) >= grid(0)
     beyond = jnp.sum(top + jnp.where(later, far, 0.0), axis=0, keepdims=True)
+    spot = lax.broadcasted_iota(jnp.int32, (1, BLK), 1)
+    clipped = jnp.where(
+        spot == (BLK - 1 + shift) % BLK, jnp.sum(beyond, axis=1, keepdims=True), 0.0
+    )
     return (
-        unshear(jnp.where(later, 0.0, near)),
-        unshear(jnp.where(later, near, far)),
-        beyond,
+        unshear(jnp.where(later, 0.0, near), shift),
+        unshear(jnp.where(later, near, far), shift) + clipped,
     )
 
 
@@ -89,11 +93,11 @@
     qd, got_qd, kv, bias_ref, square_ref, grown_ref, dprob_ref, peak_ref,
     own_k, own_v, own_q, back_q, got_q, back_kv, got_kv,
     local_stats, right_stats, halo_stats, left_stats,
-    table_rows, pieces, exchange_a, exchange_b, exchange_c, exchange_d,
+    table_rows, pieces, exchange_a, exchange_b, exchange_c,
     load_sem, hop_sem, send_sem, seq_recv, back_recv, halo_recv, misc_recv,
 ):
     if direct:
-        packs, pack_got, turns, stack = exchange_a, exchange_b, exchange_c, exchange_d
+        packs, pack_got, stack = exchange_a, exchange_b, exchange_c
     else:
         piece_got, shares = exchange_a, exchange_b
     rows, width = q_hbm.shape
@@ -113,7 +117,7 @@
 
     for p in range(pairs):
         for i, src in enumerate((q_hbm, d_hbm)):
-            pltpu.make_async_copy(src.at[:, columns(p)], qd.at[p, i], load_sem.at[2 + p]).start()
+            pltpu.make_async_copy(src.at[:, columns(p)], qd.at[p, i], load_sem.at[2 + (p > 0)]).start()
     pltpu.make_async_copy(table_hbm, table_rows, load_sem.at[0]).start()
     for p in range(pairs):
         for i, src in enumerate((k_hbm, v_hbm)):
@@ -158,36 +162,41 @@
         )
 
     def query_copy(p):
-        return remote(qd.at[p], got_qd.at[p], 0, seq_recv.at[p], left)
+        return remote(qd.at[p], got_qd.at[p], LEFTWARD, seq_recv.at[p], left)
 
     def all_queries():
-        return remote(qd.at[pl.ds(0, moved)], got_qd, 0, misc_recv.at[0], left)
+        return remote(qd.at[pl.ds(0, moved)], got_qd, LEFTWARD, misc_recv.at[0], left)
 
     def key_copy(p, block):
         return remote(
             kv.at[p, :, pl.ds(rows + block * BLK, BLK)],
             kv.at[p, :, pl.ds(block * BLK, BLK)],
-            1,
+            RIGHTWARD,
             seq_recv.at[p + block * (pairs - moved)],
             right,
         )
 
     def all_keys():
         keyed = pl.ds(moved, pairs - moved)
-        return remote(kv.at[keyed, :, own], kv.at[keyed, :, prev], 1, misc_recv.at[0], right)
+        return remote(kv.at[keyed, :, own], kv.at[keyed, :, prev], RIGHTWARD, misc_recv.at[0], right)
 
     def local_copy():
-        return remote(local_stats, right_stats, 2, misc_recv.at[0], left)
+        return remote(local_stats, right_stats, LEFTWARD, misc_recv.at[0], left)
 
     def halo_copy(p):
-        return remote(halo_stats.at[p], left_stats.at[p], 3, halo_recv.at[p], right)
+        return remote(halo_stats.at[p], left_stats.at[p], RIGHTWARD, halo_recv.at[p], right)
 
     def back_copy(p):
-        return remote(back_q.at[p], got_q.at[p], 4, back_recv.at[p], right)
+        recv = back_recv.at[int(p == moved - 1)]
+        return remote(back_q.at[p], got_q.at[p], RIGHTWARD, recv, right)
+
+    def early_back():
+        some = pl.ds(0, max(moved - 1, 1))
+        return remote(back_q.at[some], got_q.at[some], RIGHTWARD, back_recv.at[0], right)
 
     def key_back_copy(p):
         i = p - moved
-        return remote(back_kv.at[i], got_kv.at[i], 5, back_recv.at[p], left)
+        return remote(back_kv.at[i], got_kv.at[i], LEFTWARD, back_recv.at[2 + i], left)
 
     def send_queries(p):
         @pl.when(has_left)
@@ -223,13 +232,14 @@
         row = table_rows[pl.ds(col * heads + h, 1), :] * LOG2E
         build_bias(row, bias_ref, h // 2, h % 2)
 
-    for p in range(1, pairs):
-        load_wait(qd.at[p], load_sem.at[2 + p])
+    load_wait(qd.at[pl.ds(1, pairs - 1)], load_sem.at[3])
     load_wait(kv.at[:, :, own], load_sem.at[1])
 
     low = lax.broadcasted_iota(jnp.int32, (BLK, LANES), 1) < HEAD_DIM
     scale = HEAD_DIM ** -0.5
-    sums = {}
+    groups = CLIP // part
+    folded = exchange_a.shape[1]
+    wide = heads // folded
 
     def split(x):
         zero = jnp.zeros_like(x)
@@ -375,11 +385,15 @@
 
     def tally(p, square):
         for lane in range(2):
-            sums[2 * p + lane] = diagonals(square[:, lane * BLK : (lane + 1) * BLK])
-
-    def local(p):
-        cols = pl.ds(p * LANES, LANES)
-
+            head = 2 * p + lane
+            sides = diagonals(
+                square[:, lane * BLK : (lane + 1) * BLK],
+                part * (head % wide) if direct else 0,
+            )
+            for side in range(2):
+                pieces[side, head : head + 1] = sides[side]
+
+    def local_probs(p):
         @pl.when(has_left)
         def _():
             halo_copy(p).wait_recv()
@@ -402,6 +416,10 @@
             axis=0,
         )
         tally(p, square)
+        return p0, s0, p1, s1
+
+    def local_grads(p, p0, s0, p1, s1):
+        cols = columns(p)
         k0, v0, q0 = tile_grads(p, 0, False, p0, s0)
         k1, v1, q1 = tile_grads(p, 1, False, p1, s1)
         for out, ref, a, b in ((dk_ref, own_k, k0, k1), (dv_ref, own_v, v0, v1)):
@@ -410,42 +428,70 @@
         own_q[p, :BLK, :] = q0
         own_q[p, BLK:, :] = q1
 
+    def local(p):
+        local_grads(p, *local_probs(p))
+
     gate = jnp.where(has_left, 0.0, NEG_FILL)
 
-    def full(p, before=None, between=None):
-        cols = pl.ds(p * LANES, LANES)
+    def full(p, between=None):
+        cols = columns(p)
         i = p - moved
 
-        def half_probs(half):
+        def arrived(block):
             @pl.when(has_left)
             def _():
-                key_copy(p, half).wait_recv()
-
-            keys = pl.ds(half * BLK, BAND)
+                key_copy(p, block).wait_recv()
+
+        def part_of(half, row, size, before):
+            keys = pl.ds(half * BLK + row, size)
             qq, dd = queries(qd, p, half)
-            scores = dot(kv[p, 0, keys], qq, NT) * LOG2E + bias_ref[p]
-            before = REACH - half * BLK
-            scores = jnp.concatenate([scores[:before] + gate, scores[before:]], axis=0)
-            dprobs = dot(kv[p, 1, keys], dd, NT)
+            scores = dot(kv[p, 0, keys], qq, NT) * LOG2E + bias_ref[p, pl.ds(row, size)]
+            scores = (
+                jnp.concatenate([scores[:before] + gate, scores[before:]], axis=0)
+                if before < size
+                else scores + gate
+            )
             peak = jnp.max(scores, axis=0, keepdims=True)
-            grown = jnp.exp2(scores - peak)
-            inverse = 1.0 / jnp.sum(grown, axis=0, keepdims=True)
-            inner = jnp.sum(grown * dprobs, axis=0, keepdims=True) * inverse
-            probs = grown * inverse
-            return probs, probs * (dprobs - inner)
+            return scores, dot(kv[p, 1, keys], dd, NT), peak
+
+        def moments(grown, dprobs):
+            return (
+                jnp.sum(grown, axis=0, keepdims=True),
+                jnp.sum(grown * dprobs, axis=0, keepdims=True),
+            )
 
         def half_grads(half, probs, dscores):
             qq, dd = queries(qd, p, half)
             return products(kv[p, 0, pl.ds(half * BLK, BAND)], qq, dd, probs, dscores)
 
-        p1, s1 = half_probs(1)
-        k1, v1, q1 = half_grads(1, p1, s1)
-        if before is not None:
-            before()
-        p0, s0 = half_probs(0)
+        arrived(1)
+        scores, dprobs, peak = part_of(1, 0, BAND, BLK)
+        grown = jnp.exp2(scores - peak)
+        total, inner = moments(grown, dprobs)
+        inverse = 1.0 / total
+        probs = grown * inverse
+        s1 = probs * (dprobs - inner * inverse)
+        k1, v1, q1 = half_grads(1, probs, s1)
+        scores_a, dprobs_a, peak_a = part_of(0, BLK, 2 * BLK, BLK)
+        grown_a = jnp.exp2(scores_a - peak_a)
+        total_a, inner_a = moments(grown_a, dprobs_a)
+
+        arrived(0)
+        scores_b, dprobs_b, peak_b = part_of(0, 0, BLK, BLK)
+        peak = jnp.maximum(peak_a, peak_b)
+        grown_b = jnp.exp2(scores_b - peak)
+        total_b, inner_b = moments(grown_b, dprobs_b)
+        factor = jnp.exp2(peak_a - peak)
+        inverse = 1.0 / (total_a * factor + total_b)
+        inner = (inner_a * factor + inner_b) * inverse
+        probs_a, probs_b = grown_a * (factor * inverse), grown_b * inverse
+        p0 = jnp.concatenate([probs_b, probs_a], axis=0)
+        s0 = jnp.concatenate(
+            [probs_b * (dprobs_b - inner), probs_a * (dprobs_a - inner)], axis=0
+        )
+        tally(p, s0 + s1)
         if p == pairs - 1:
             send_back(moved - 1)
-        tally(p, s0 + s1)
         if between is not None:
             between()
         k0, v0, q0 = half_grads(0, p0, s0)
@@ -466,7 +512,7 @@
         return pltpu.make_async_remote_copy(
             src_ref=src,
             dst_ref=dst,
-            send_sem=send_sem.at[6],
+            send_sem=send_sem.at[2],
             recv_sem=misc_recv.at[1],
             device_id=(target, lax.rem(col + t, tp_size)),
             device_id_type=MESH,
@@ -474,13 +520,13 @@
 
     def all_pieces():
         ref = pack_got.at[pl.ds(1, sp_size * tp_size - 1)] if direct else piece_got
-        return remote(ref, ref, 6, misc_recv.at[1], left)
+        return remote(ref, ref, 2, misc_recv.at[1], left)
 
     def share_copy(k):
         return pltpu.make_async_remote_copy(
             src_ref=shares.at[0],
             dst_ref=shares.at[k],
-            send_sem=send_sem.at[7],
+            send_sem=send_sem.at[3],
             recv_sem=misc_recv.at[2],
             device_id=(me, lax.rem(col + k, tp_size)),
             device_id_type=MESH,
@@ -488,22 +534,16 @@
 
     def all_shares():
         rest = shares.at[pl.ds(1, tp_size - 1)]
-        return remote(rest, rest, 7, misc_recv.at[2], left)
-
-    groups = CLIP // part
-    folded = exchange_a.shape[1]
-    wide = heads // folded
+        return remote(rest, rest, 3, misc_recv.at[2], left)
 
     def fold():
         block = lax.broadcasted_iota(jnp.int32, (folded, CLIP), 1) // part
         for side in range(2):
-            for a in range(groups):
-                turns[a] = turned(pieces[side], part * a)
+            lines = [pieces[side, pl.ds(j, folded, stride=wide), :] for j in range(wide)]
             for m in range(groups):
                 pack = jnp.zeros((folded, CLIP), F32)
                 for j in range(wide):
-                    line = turns[(j - m) % groups, pl.ds(j, folded, stride=wide), :]
-                    pack = jnp.where(block == j, line, pack)
+                    pack = jnp.where(block == (m + j) % groups, lines[j], pack)
                 packs[side * groups + m] = pack
 
     def unfold():
@@ -515,19 +555,15 @@
             total.append(line)
         total = jnp.concatenate(total, axis=0)
         for j in range(wide):
-            stack[pl.ds(j, folded * tp_size, stride=wide), :] = turned(total, -part * j)
+            away = lax.rem(me + j, groups) * part
+            stack[pl.ds(j, folded * tp_size, stride=wide), :] = pltpu.roll(
+                total, lax.rem(CLIP - away, CLIP), 1
+            )
         dt_ref[...] = jnp.transpose(stack[...])[:part]
 
     def send_pieces():
         for r in range(moved + 1, rounds + 1):
             hop(r)
-        behind, ahead, beyond = (
-            jnp.concatenate([sums[h][i] for h in range(heads)], axis=0) for i in range(3)
-        )
-        beyond = jnp.sum(beyond, axis=1, keepdims=True)
-        spot = lax.broadcasted_iota(jnp.int32, (heads, BLK), 1)
-        pieces[0] = behind
-        pieces[1] = ahead + jnp.where(spot == BLK - 1, beyond, 0.0)
         if direct:
             fold()
             pack_got[col * sp_size + me] = packs[me]
@@ -548,18 +584,27 @@
         send_back(p)
         if p == moved:
             local(moved - 1)
-    if moved < last:
-        full(last, None, send_pieces)
-    else:
-        full(last, lambda: local(moved - 1), send_pieces)
+    kept = []
+
+    def finish_pieces():
+        if moved == last:
+            kept.extend(local_probs(moved - 1))
+        send_pieces()
+
+    full(last, finish_pieces)
     send_back(last)
+    if kept:
+        local_grads(moved - 1, *kept)
 
     def finish(p):
         cols = pl.ds(p * LANES, LANES)
         if p < moved:
             @pl.when(has_left)
             def _():
-                back_copy(p).wait_recv()
+                if p == moved - 1:
+                    back_copy(p).wait_recv()
+                elif p == 0:
+                    early_back().wait_recv()
                 dq_ref[:, cols] = (own_q[p] + got_q[p].astype(F32)).astype(BF16)
 
             @pl.when(jnp.logical_not(has_left))
@@ -579,8 +624,9 @@
                 dk_ref[:, cols] = own_k[p].astype(BF16)
                 dv_ref[:, cols] = own_v[p].astype(BF16)
 
-    for p in range(moved - 1):
-        finish(p)
+    if direct:
+        for p in range(pairs):
+            finish(p)
     all_pieces().wait_recv()
     if direct:
         unfold()
@@ -591,9 +637,9 @@
         shares[0] = pltpu.roll(total, lax.rem(CLIP - lax.rem(me * part, CLIP), CLIP), 1)
         for k in range(1, tp_size):
             share_copy(k).start()
-    for p in range(moved - 1, pairs):
-        finish(p)
     if not direct:
+        for p in range(pairs):
+            finish(p)
         all_shares().wait_recv()
         stacked = jnp.concatenate(
             [shares[lax.rem(col + tp_size - t, tp_size)] for t in range(tp_size)], axis=0
@@ -607,13 +653,13 @@
     def _():
         all_queries().wait_send()
         local_copy().wait_send()
-        remote(back_kv, got_kv, 5, misc_recv.at[0], left).wait_send()
+        remote(back_kv, got_kv, LEFTWARD, misc_recv.at[0], left).wait_send()
 
     @pl.when(has_right)
     def _():
         all_keys().wait_send()
-        remote(halo_stats, left_stats, 3, misc_recv.at[0], right).wait_send()
-        remote(back_q, got_q, 4, misc_recv.at[0], right).wait_send()
+        remote(halo_stats, left_stats, RIGHTWARD, misc_recv.at[0], right).wait_send()
+        remote(back_q, got_q, RIGHTWARD, misc_recv.at[0], right).wait_send()
 
 
 def shards(sp_size, tp_size, query_rows, key_rows, value_rows, out_grad, rel_bias):
@@ -631,11 +677,10 @@
             (
                 (sp_size, folded, CLIP),
                 (sp_size * tp_size, folded, CLIP),
-                (CLIP // part, heads, CLIP),
                 (tp_size * heads, CLIP),
             )
             if direct
-            else ((sp_size - 1, heads, CLIP), (tp_size, heads, CLIP), (8, CLIP), (8, CLIP))
+            else ((sp_size - 1, heads, CLIP), (tp_size, heads, CLIP), (8, CLIP))
         )
     ]
     assert rows == REACH and REACH == 2 * BLK and CLIP == BLK
@@ -670,13 +715,13 @@
             pltpu.VMEM(rel_bias.shape[::-1], F32),
             pltpu.VMEM((2, heads, BLK), F32),
             *exchange,
-            dma((2 + pairs,)),
+            dma((4,)),
             pltpu.SemaphoreType.REGULAR((rounds + 1,)),
-            dma((8,)),
+            dma((3 if direct else 4,)),
             dma((2 * pairs - moved,)),
-            dma((pairs,)),
+            dma((2 + pairs - moved,)),
             dma((moved,)),
-            dma((3,)),
+            dma((2 if direct else 3,)),
         ],
         compiler_params=pltpu.CompilerParams(
             collective_id=0, has_side_effects=True, vmem_limit_bytes=48 * 1024 * 1024

time: 27.9 us -> 27.4 us (0.982)
  Pallas kernels: 27.1 us -> 26.6 us
    pallas_call x1, Pallas kernels: 26.2 us -> 25.7 us  [shards(): pl.pallas_call(partial(kernel, sp_size, tp_size, moved, direct), out_shap...]
where the time goes in v3:
time: 27.4 us; the launch traced here: 27.3 us
  Pallas kernels  26.6 us (97%)
  between operations  0.64 us (2%)
    pallas_call x1, Pallas kernels, shards(): pl.pallas_call(partial(kernel, sp_size, tp_size, moved, direct), out_shap...  25.7 us
    pallas_call x1, Pallas kernels, shards(): pl.pallas_call(write_out, out_shape=shapes, in_specs=[pl.BlockSpec(memory...  0.91 us

profile of v3, /device:TPU:0, one launch (start us, length us, event | category | flops | bytes accessed | tf_op | source)
XLA Modules:
  0.0 27.3 jit_solution(2538782972160356209)
XLA Ops:
  0.6 25.7 %shard_map.84 = (bf16[256,512]{1,0:T(8,128)(2,1)S(1)}, bf16[256,512]{1,0:T(8,128)(2,1)S(1)}, bf16[256,512]{1,0:T(8,128)(2,1)S(1)}, f32[32,32]{1,0:T(8,128)S(1)}) custom-call(bf16[256,512]{1,0:T(8,128)(2,1)} %q_hbm.1, bf16[256,512]{1,0:T(8,128)(2,1)} %k_hbm.1, bf16[256,512]{1,0:T(8,128)(2,1)} %v_hbm.1, bf16[256,512]{1,0:T(8,128)(2,1)} %d_hbm.1, f32[32,256]{1,0:T(8,128)} %bitcast.1), custom_call_target="tpu_custom_call" | custom-call | tf_op jit(solution)/shard_map/pallas_call | solution.py:690
  26.3 0.9 %shard_map.85 = (bf16[256,512]{1,0:T(8,128)(2,1)}, bf16[256,512]{1,0:T(8,128)(2,1)}, bf16[256,512]{1,0:T(8,128)(2,1)}, f32[32,32]{1,0:T(8,128)}) custom-call(bf16[256,512]{1,0:T(8,128)(2,1)S(1)} %get-tuple-element.8.refs_0_, bf16[256,512]{1,0:T(8,128)(2,1)S(1)} %get-tuple-element.9.refs_1_, bf16[256,512]{1,0:T(8,128)(2,1)S(1)} %get-tuple-element.10.refs_2_, ...), custom_call_target="tpu_custom_call" | custom-call | tf_op jit(solution)/shard_map/pallas_call | solution.py:730

commit v4 on v3

--- a/solution.py
+++ b/solution.py
@@ -115,6 +115,29 @@
     def columns(p):
         return pl.ds(p * LANES, LANES)
 
+    barrier = pltpu.get_barrier_semaphore()
+
+    def greet(sem, step):
+        @pl.when(me >= step)
+        def _():
+            pl.semaphore_signal(sem, inc=1, device_id=(me - step, col), device_id_type=MESH)
+
+        @pl.when(me + step < sp_size)
+        def _():
+            pl.semaphore_signal(sem, inc=1, device_id=(me + step, col), device_id_type=MESH)
+
+    def greeters(step):
+        return (me >= step).astype(jnp.int32) + (me + step < sp_size).astype(jnp.int32)
+
+    @pl.when(has_right)
+    def _():
+        pl.semaphore_signal(barrier, inc=1, device_id=(me + 1, col), device_id_type=MESH)
+
+    for k in range(1, tp_size):
+        pl.semaphore_signal(
+            barrier, inc=1, device_id=(me, lax.rem(col + k, tp_size)), device_id_type=MESH
+        )
+
     for p in range(pairs):
         for i, src in enumerate((q_hbm, d_hbm)):
             pltpu.make_async_copy(src.at[:, columns(p)], qd.at[p, i], load_sem.at[2 + (p > 0)]).start()
@@ -122,26 +145,6 @@
     for p in range(pairs):
         for i, src in enumerate((k_hbm, v_hbm)):
             pltpu.make_async_copy(src.at[:, columns(p)], kv.at[p, i, own], load_sem.at[1]).start()
-
-    barrier = pltpu.get_barrier_semaphore()
-
-    def greet(sem, step):
-        @pl.when(me >= step)
-        def _():
-            pl.semaphore_signal(sem, inc=1, device_id=(me - step, col), device_id_type=MESH)
-
-        @pl.when(me + step < sp_size)
-        def _():
-            pl.semaphore_signal(sem, inc=1, device_id=(me + step, col), device_id_type=MESH)
-
-    def greeters(step):
-        return (me >= step).astype(jnp.int32) + (me + step < sp_size).astype(jnp.int32)
-
-    greet(barrier, 1)
-    for k in range(1, tp_size):
-        pl.semaphore_signal(
-            barrier, inc=1, device_id=(me, lax.rem(col + k, tp_size)), device_id_type=MESH
-        )
 
     rounds = hop_sem.shape[0] - 1
 
@@ -164,6 +167,13 @@
     def query_copy(p):
         return remote(qd.at[p], got_qd.at[p], LEFTWARD, seq_recv.at[p], left)
 
+    turn = max(moved - 2, 0)
+
+    def query_part(half):
+        mine = pl.ds(half * BLK, BLK)
+        recv = seq_recv.at[2 * pairs - moved if half == 0 else turn]
+        return remote(qd.at[turn, :, mine], got_qd.at[turn, :, mine], LEFTWARD, recv, left)
+
     def all_queries():
         return remote(qd.at[pl.ds(0, moved)], got_qd, LEFTWARD, misc_recv.at[0], left)
 
@@ -201,7 +211,11 @@
     def send_queries(p):
         @pl.when(has_left)
         def _():
-            query_copy(p).start()
+            if p == turn:
+                query_part(1).start()
+                query_part(0).start()
+            else:
+                query_copy(p).start()
 
     def send_back(p):
         if p < moved:
@@ -216,10 +230,9 @@
     def load_wait(refs, sem):
         pltpu.make_async_copy(refs, refs, sem).wait()
 
-    pl.semaphore_wait(barrier, greeters(1) + tp_size - 1)
+    pl.semaphore_wait(barrier, has_left.astype(jnp.int32) + tp_size - 1)
     load_wait(qd.at[0], load_sem.at[2])
     send_queries(0)
-    hop(0)
 
     @pl.when(jnp.logical_not(has_left))
     def _():
@@ -322,41 +335,51 @@
     core = lax.rem(col, 2)
     early = has_right & (even | (core == 0))
     keyed = [(p, block) for p in range(moved, pairs) for block in (1, 0)]
-    turn = moved - 2 if moved > 1 else 0
-
-    def send_keys():
-        for p, block in keyed:
+
+    def send_keys(blocks):
+        for p, block in blocks:
             key_copy(p, block).start()
+
+    def first_keys():
+        @pl.when(has_right & jnp.logical_not(even) & (core == 0))
+        def _():
+            pl.semaphore_signal(
+                hop_sem.at[rounds], inc=1, device_id=(me, col + 1), device_id_type=MESH
+            )
+
+        @pl.when(early)
+        def _():
+            send_keys(keyed[:1])
 
     def after_stats(p):
         if p + 2 < moved:
             send_queries(p + 2)
         if p == turn:
-            @pl.when(has_right & jnp.logical_not(even) & (core == 0))
-            def _():
-                pl.semaphore_signal(
-                    hop_sem.at[rounds], inc=1, device_id=(me, col + 1), device_id_type=MESH
-                )
-
             @pl.when(early)
             def _():
-                send_keys()
+                send_keys(keyed[1:])
+
+            @pl.when(has_right & jnp.logical_not(early))
+            def _():
+                pl.semaphore_wait(hop_sem.at[rounds], 1)
+                send_keys(keyed)
 
         if p == moved - 1:
             for done in range(p):
                 send_back(done)
 
-    def late_keys():
-        @pl.when(has_right & jnp.logical_not(early))
-        def _():
-            pl.semaphore_wait(hop_sem.at[rounds], 1)
-            send_keys()
-
     def halo(p):
         @pl.when(has_right)
         def _():
-            query_copy(p).wait_recv()
-            kept = [partial_softmax(p, half, True, halo_stats) for half in range(2)]
+            if p == turn:
+                query_part(1).wait_recv()
+                kept = [partial_softmax(p, 1, True, halo_stats)]
+                query_part(0).wait_recv()
+                first_keys()
+                kept.insert(0, partial_softmax(p, 0, True, halo_stats))
+            else:
+                query_copy(p).wait_recv()
+                kept = [partial_softmax(p, half, True, halo_stats) for half in range(2)]
             halo_copy(p).start()
             after_stats(p)
             if p == 0:
@@ -381,7 +404,7 @@
             own_v[p] = jnp.zeros((rows, LANES), F32)
             square_ref[p, :REACH, :] = jnp.zeros((REACH, 2 * BLK), F32)
 
-        hop(p + 1)
+        hop(p)
 
     def tally(p, square):
         for lane in range(2):
@@ -562,7 +585,7 @@
         dt_ref[...] = jnp.transpose(stack[...])[:part]
 
     def send_pieces():
-        for r in range(moved + 1, rounds + 1):
+        for r in range(moved, rounds + 1):
             hop(r)
         if direct:
             fold()
@@ -576,8 +599,6 @@
         halo(p)
         if p:
             local(p - 1)
-        if p == turn:
-            late_keys()
     last = pairs - 1
     for p in range(moved, last):
         full(p)
@@ -718,7 +739,7 @@
             dma((4,)),
             pltpu.SemaphoreType.REGULAR((rounds + 1,)),
             dma((3 if direct else 4,)),
-            dma((2 * pairs - moved,)),
+            dma((2 * pairs - moved + 1,)),
             dma((2 + pairs - moved,)),
             dma((moved,)),
             dma((2 if direct else 3,)),

time: 27.4 us -> 26.9 us (0.982)
  Pallas kernels: 26.6 us -> 26.1 us
    pallas_call x1, Pallas kernels: 25.7 us -> 25.2 us  [shards(): pl.pallas_call(partial(kernel, sp_size, tp_size, moved, direct), out_shap...]
where the time goes in v4:
time: 26.9 us; the launch traced here: 26.7 us
  Pallas kernels  26.1 us (97%)
  between operations  0.64 us (2%)
    pallas_call x1, Pallas kernels, shards(): pl.pallas_call(partial(kernel, sp_size, tp_size, moved, direct), out_shap...  25.2 us
    pallas_call x1, Pallas kernels, shards(): pl.pallas_call(write_out, out_shape=shapes, in_specs=[pl.BlockSpec(memory...  0.91 us

profile of v4, /device:TPU:0, one launch (start us, length us, event | category | flops | bytes accessed | tf_op | source)
XLA Modules:
  0.0 26.7 jit_solution(3946128259080498234)
XLA Ops:
  0.6 25.2 %shard_map.84 = (bf16[256,512]{1,0:T(8,128)(2,1)S(1)}, bf16[256,512]{1,0:T(8,128)(2,1)S(1)}, bf16[256,512]{1,0:T(8,128)(2,1)S(1)}, f32[32,32]{1,0:T(8,128)S(1)}) custom-call(bf16[256,512]{1,0:T(8,128)(2,1)} %q_hbm.1, bf16[256,512]{1,0:T(8,128)(2,1)} %k_hbm.1, bf16[256,512]{1,0:T(8,128)(2,1)} %v_hbm.1, bf16[256,512]{1,0:T(8,128)(2,1)} %d_hbm.1, f32[32,256]{1,0:T(8,128)} %bitcast.1), custom_call_target="tpu_custom_call" | custom-call | tf_op jit(solution)/shard_map/pallas_call | solution.py:711
  25.8 0.9 %shard_map.85 = (bf16[256,512]{1,0:T(8,128)(2,1)}, bf16[256,512]{1,0:T(8,128)(2,1)}, bf16[256,512]{1,0:T(8,128)(2,1)}, f32[32,32]{1,0:T(8,128)}) custom-call(bf16[256,512]{1,0:T(8,128)(2,1)S(1)} %get-tuple-element.8.refs_0_, bf16[256,512]{1,0:T(8,128)(2,1)S(1)} %get-tuple-element.9.refs_1_, bf16[256,512]{1,0:T(8,128)(2,1)S(1)} %get-tuple-element.10.refs_2_, ...), custom_call_target="tpu_custom_call" | custom-call | tf_op jit(solution)/shard_map/pallas_call | solution.py:751

commit v5 on v4

--- a/solution.py
+++ b/solution.py
@@ -167,11 +167,11 @@
     def query_copy(p):
         return remote(qd.at[p], got_qd.at[p], LEFTWARD, seq_recv.at[p], left)
 
-    turn = max(moved - 2, 0)
+    turn, last = max(moved - 2, 0), pairs - 1
 
     def query_part(half):
-        mine = pl.ds(half * BLK, BLK)
-        recv = seq_recv.at[2 * pairs - moved if half == 0 else turn]
+        mine = pl.ds(SEG, rows - SEG) if half else pl.ds(0, SEG)
+        recv = seq_recv.at[turn if half else 2 * pairs - moved]
         return remote(qd.at[turn, :, mine], got_qd.at[turn, :, mine], LEFTWARD, recv, left)
 
     def all_queries():
@@ -374,14 +374,15 @@
             if p == turn:
                 query_part(1).wait_recv()
                 kept = [partial_softmax(p, 1, True, halo_stats)]
+                first_keys()
                 query_part(0).wait_recv()
-                first_keys()
                 kept.insert(0, partial_softmax(p, 0, True, halo_stats))
             else:
                 query_copy(p).wait_recv()
                 kept = [partial_softmax(p, half, True, halo_stats) for half in range(2)]
             halo_copy(p).start()
             after_stats(p)
+            hop(p)
             if p == 0:
                 local_copy().wait_recv()
             (p0, s0), (p1, s1) = (
@@ -400,11 +401,10 @@
         @pl.when(jnp.logical_not(has_right))
         def _():
             after_stats(p)
+            hop(p)
             own_k[p] = jnp.zeros((rows, LANES), F32)
             own_v[p] = jnp.zeros((rows, LANES), F32)
             square_ref[p, :REACH, :] = jnp.zeros((REACH, 2 * BLK), F32)
-
-        hop(p)
 
     def tally(p, square):
         for lane in range(2):
@@ -599,7 +599,6 @@
         halo(p)
         if p:
             local(p - 1)
-    last = pairs - 1
     for p in range(moved, last):
         full(p)
         send_back(p)

time: 26.9 us -> 26.4 us (0.981)
  Pallas kernels: 26.1 us -> 25.6 us
    pallas_call x1, Pallas kernels: 25.2 us -> 24.7 us  [shards(): pl.pallas_call(partial(kernel, sp_size, tp_size, moved, direct), out_shap...]
where the time goes in v5:
time: 26.4 us; the launch traced here: 26.3 us
  Pallas kernels  25.6 us (97%)
  between operations  0.64 us (2%)
    pallas_call x1, Pallas kernels, shards(): pl.pallas_call(partial(kernel, sp_size, tp_size, moved, direct), out_shap...  24.7 us
    pallas_call x1, Pallas kernels, shards(): pl.pallas_call(write_out, out_shape=shapes, in_specs=[pl.BlockSpec(memory...  0.91 us

profile of v5, /device:TPU:0, one launch (start us, length us, event | category | flops | bytes accessed | tf_op | source)
XLA Modules:
  0.0 26.3 jit_solution(7889783852319203198)
XLA Ops:
  0.6 24.7 %shard_map.84 = (bf16[256,512]{1,0:T(8,128)(2,1)S(1)}, bf16[256,512]{1,0:T(8,128)(2,1)S(1)}, bf16[256,512]{1,0:T(8,128)(2,1)S(1)}, f32[32,32]{1,0:T(8,128)S(1)}) custom-call(bf16[256,512]{1,0:T(8,128)(2,1)} %q_hbm.1, bf16[256,512]{1,0:T(8,128)(2,1)} %k_hbm.1, bf16[256,512]{1,0:T(8,128)(2,1)} %v_hbm.1, bf16[256,512]{1,0:T(8,128)(2,1)} %d_hbm.1, f32[32,256]{1,0:T(8,128)} %bitcast.1), custom_call_target="tpu_custom_call" | custom-call | tf_op jit(solution)/shard_map/pallas_call | solution.py:710
  25.3 0.9 %shard_map.85 = (bf16[256,512]{1,0:T(8,128)(2,1)}, bf16[256,512]{1,0:T(8,128)(2,1)}, bf16[256,512]{1,0:T(8,128)(2,1)}, f32[32,32]{1,0:T(8,128)}) custom-call(bf16[256,512]{1,0:T(8,128)(2,1)S(1)} %get-tuple-element.8.refs_0_, bf16[256,512]{1,0:T(8,128)(2,1)S(1)} %get-tuple-element.9.refs_1_, bf16[256,512]{1,0:T(8,128)(2,1)S(1)} %get-tuple-element.10.refs_2_, ...), custom_call_target="tpu_custom_call" | custom-call | tf_op jit(solution)/shard_map/pallas_call | solution.py:750

commit v6 on v5

--- a/solution.py
+++ b/solution.py
@@ -138,13 +138,13 @@
             barrier, inc=1, device_id=(me, lax.rem(col + k, tp_size)), device_id_type=MESH
         )
 
-    for p in range(pairs):
+    def load_queries(p):
         for i, src in enumerate((q_hbm, d_hbm)):
-            pltpu.make_async_copy(src.at[:, columns(p)], qd.at[p, i], load_sem.at[2 + (p > 0)]).start()
+            sem = load_sem.at[2 + (p > 0)]
+            pltpu.make_async_copy(src.at[:, columns(p)], qd.at[p, i], sem).start()
+
+    load_queries(0)
     pltpu.make_async_copy(table_hbm, table_rows, load_sem.at[0]).start()
-    for p in range(pairs):
-        for i, src in enumerate((k_hbm, v_hbm)):
-            pltpu.make_async_copy(src.at[:, columns(p)], kv.at[p, i, own], load_sem.at[1]).start()
 
     rounds = hop_sem.shape[0] - 1
 
@@ -197,16 +197,14 @@
         return remote(halo_stats.at[p], left_stats.at[p], RIGHTWARD, halo_recv.at[p], right)
 
     def back_copy(p):
-        recv = back_recv.at[int(p == moved - 1)]
-        return remote(back_q.at[p], got_q.at[p], RIGHTWARD, recv, right)
-
-    def early_back():
-        some = pl.ds(0, max(moved - 1, 1))
-        return remote(back_q.at[some], got_q.at[some], RIGHTWARD, back_recv.at[0], right)
+        return remote(back_q.at[p], got_q.at[p], RIGHTWARD, back_recv.at[0], right)
+
+    def all_back():
+        return remote(back_q, got_q, RIGHTWARD, back_recv.at[0], right)
 
     def key_back_copy(p):
         i = p - moved
-        return remote(back_kv.at[i], got_kv.at[i], LEFTWARD, back_recv.at[2 + i], left)
+        return remote(back_kv.at[i], got_kv.at[i], LEFTWARD, back_recv.at[1 + i], left)
 
     def send_queries(p):
         @pl.when(has_left)
@@ -233,6 +231,11 @@
     pl.semaphore_wait(barrier, has_left.astype(jnp.int32) + tp_size - 1)
     load_wait(qd.at[0], load_sem.at[2])
     send_queries(0)
+    for p in range(1, pairs):
+        load_queries(p)
+    for p in range(pairs):
+        for i, src in enumerate((k_hbm, v_hbm)):
+            pltpu.make_async_copy(src.at[:, columns(p)], kv.at[p, i, own], load_sem.at[1]).start()
 
     @pl.when(jnp.logical_not(has_left))
     def _():
@@ -526,8 +529,7 @@
         dq_ref[:BLK, cols] = q0.astype(BF16)
         dq_ref[BLK:, cols] = q1.astype(BF16)
 
-    def piece_copy(k, t):
-        target = lax.rem(me + k, sp_size)
+    def piece_copy(target, t, k=1):
         if direct:
             src, dst = packs.at[target], pack_got.at[col * sp_size + me]
         else:
@@ -570,6 +572,7 @@
                 packs[side * groups + m] = pack
 
     def unfold():
+        pack_got[col * sp_size + me] = packs[me]
         total = []
         for t in range(tp_size):
             line = pack_got[t * sp_size]
@@ -589,11 +592,14 @@
             hop(r)
         if direct:
             fold()
-            pack_got[col * sp_size + me] = packs[me]
-        for k in range(sp_size):
-            for t in range(tp_size if direct else 1):
-                if k or t:
-                    piece_copy(k, t).start()
+        beside = range(1, tp_size if direct else 1)
+        for t in beside:
+            piece_copy(0, t).start()
+        for k in range(1, sp_size):
+            piece_copy(lax.rem(me + k, sp_size), 0, k).start()
+        for target in range(1, sp_size):
+            for t in beside:
+                piece_copy(target, t).start()
 
     for p in range(moved):
         halo(p)
@@ -621,10 +627,8 @@
         if p < moved:
             @pl.when(has_left)
             def _():
-                if p == moved - 1:
-                    back_copy(p).wait_recv()
-                elif p == 0:
-                    early_back().wait_recv()
+                if p == 0:
+                    all_back().wait_recv()
                 dq_ref[:, cols] = (own_q[p] + got_q[p].astype(F32)).astype(BF16)
 
             @pl.when(jnp.logical_not(has_left))
@@ -679,7 +683,7 @@
     def _():
         all_keys().wait_send()
         remote(halo_stats, left_stats, RIGHTWARD, misc_recv.at[0], right).wait_send()
-        remote(back_q, got_q, RIGHTWARD, misc_recv.at[0], right).wait_send()
+        all_back().wait_send()
 
 
 def shards(sp_size, tp_size, query_rows, key_rows, value_rows, out_grad, rel_bias):
@@ -739,7 +743,7 @@
             pltpu.SemaphoreType.REGULAR((rounds + 1,)),
             dma((3 if direct else 4,)),
             dma((2 * pairs - moved + 1,)),
-            dma((2 + pairs - moved,)),
+            dma((1 + pairs - moved,)),
             dma((moved,)),
             dma((2 if direct else 3,)),
         ],

time: 26.4 us -> 26.3 us (level)
  no operation moved by 1% of the time
where the time goes in v6:
time: 26.3 us; the launch traced here: 26.1 us
  Pallas kernels  25.4 us (97%)
  between operations  0.64 us (2%)
    pallas_call x1, Pallas kernels, shards(): pl.pallas_call(partial(kernel, sp_size, tp_size, moved, direct), out_shap...  24.5 us
    pallas_call x1, Pallas kernels, shards(): pl.pallas_call(write_out, out_shape=shapes, in_specs=[pl.BlockSpec(memory...  0.91 us

profile of v6, /device:TPU:0, one launch (start us, length us, event | category | flops | bytes accessed | tf_op | source)
XLA Modules:
  0.0 26.1 jit_solution(743231705961960974)
XLA Ops:
  0.6 24.5 %shard_map.84 = (bf16[256,512]{1,0:T(8,128)(2,1)S(1)}, bf16[256,512]{1,0:T(8,128)(2,1)S(1)}, bf16[256,512]{1,0:T(8,128)(2,1)S(1)}, f32[32,32]{1,0:T(8,128)S(1)}) custom-call(bf16[256,512]{1,0:T(8,128)(2,1)} %q_hbm.1, bf16[256,512]{1,0:T(8,128)(2,1)} %k_hbm.1, bf16[256,512]{1,0:T(8,128)(2,1)} %v_hbm.1, bf16[256,512]{1,0:T(8,128)(2,1)} %d_hbm.1, f32[32,256]{1,0:T(8,128)} %bitcast.1), custom_call_target="tpu_custom_call" | custom-call | tf_op jit(solution)/shard_map/pallas_call | solution.py:714
  25.1 0.9 %shard_map.85 = (bf16[256,512]{1,0:T(8,128)(2,1)}, bf16[256,512]{1,0:T(8,128)(2,1)}, bf16[256,512]{1,0:T(8,128)(2,1)}, f32[32,32]{1,0:T(8,128)}) custom-call(bf16[256,512]{1,0:T(8,128)(2,1)S(1)} %get-tuple-element.8.refs_0_, bf16[256,512]{1,0:T(8,128)(2,1)S(1)} %get-tuple-element.9.refs_1_, bf16[256,512]{1,0:T(8,128)(2,1)S(1)} %get-tuple-element.10.refs_2_, ...), custom_call_target="tpu_custom_call" | custom-call | tf_op jit(solution)/shard_map/pallas_call | solution.py:754

commit v7 on v6

--- a/solution.py
+++ b/solution.py
@@ -21,7 +21,7 @@
 NEG_FILL = -1e30
 LOG2E = math.log2(math.e)
 MESH = pl.DeviceIdType.MESH
-LEFTWARD, RIGHTWARD = 0, 1
+LEFTWARD, RIGHTWARD, PIECES, SHARES = 2, 0, 1, 3
 F32 = jnp.float32
 BF16 = jnp.bfloat16
 
@@ -94,7 +94,7 @@
     own_k, own_v, own_q, back_q, got_q, back_kv, got_kv,
     local_stats, right_stats, halo_stats, left_stats,
     table_rows, pieces, exchange_a, exchange_b, exchange_c,
-    load_sem, hop_sem, send_sem, seq_recv, back_recv, halo_recv, misc_recv,
+    load_sem, hop_sem, seq_recv, back_recv, halo_recv, misc_recv,
 ):
     if direct:
         packs, pack_got, stack = exchange_a, exchange_b, exchange_c
@@ -158,7 +158,7 @@
         return pltpu.make_async_remote_copy(
             src_ref=src,
             dst_ref=dst,
-            send_sem=send_sem.at[send],
+            send_sem=load_sem.at[send],
             recv_sem=recv,
             device_id=(target, col),
             device_id_type=MESH,
@@ -537,7 +537,7 @@
         return pltpu.make_async_remote_copy(
             src_ref=src,
             dst_ref=dst,
-            send_sem=send_sem.at[2],
+            send_sem=load_sem.at[PIECES],
             recv_sem=misc_recv.at[1],
             device_id=(target, lax.rem(col + t, tp_size)),
             device_id_type=MESH,
@@ -545,13 +545,13 @@
 
     def all_pieces():
         ref = pack_got.at[pl.ds(1, sp_size * tp_size - 1)] if direct else piece_got
-        return remote(ref, ref, 2, misc_recv.at[1], left)
+        return remote(ref, ref, PIECES, misc_recv.at[1], left)
 
     def share_copy(k):
         return pltpu.make_async_remote_copy(
             src_ref=shares.at[0],
             dst_ref=shares.at[k],
-            send_sem=send_sem.at[3],
+            send_sem=load_sem.at[SHARES],
             recv_sem=misc_recv.at[2],
             device_id=(me, lax.rem(col + k, tp_size)),
             device_id_type=MESH,
@@ -559,7 +559,7 @@
 
     def all_shares():
         rest = shares.at[pl.ds(1, tp_size - 1)]
-        return remote(rest, rest, 3, misc_recv.at[2], left)
+        return remote(rest, rest, SHARES, misc_recv.at[2], left)
 
     def fold():
         block = lax.broadcasted_iota(jnp.int32, (folded, CLIP), 1) // part
@@ -741,7 +741,6 @@
             *exchange,
             dma((4,)),
             pltpu.SemaphoreType.REGULAR((rounds + 1,)),
-            dma((3 if direct else 4,)),
             dma((2 * pairs - moved + 1,)),
             dma((1 + pairs - moved,)),
             dma((moved,)),

time: 26.3 us -> 26.2 us (level)
  no operation moved by 1% of the time
where the time goes in v7:
time: 26.2 us; the launch traced here: 26 us
  Pallas kernels  25.4 us (97%)
  between operations  0.64 us (2%)
    pallas_call x1, Pallas kernels, shards(): pl.pallas_call(partial(kernel, sp_size, tp_size, moved, direct), out_shap...  24.5 us
    pallas_call x1, Pallas kernels, shards(): pl.pallas_call(write_out, out_shape=shapes, in_specs=[pl.BlockSpec(memory...  0.91 us

profile of v7, /device:TPU:0, one launch (start us, length us, event | category | flops | bytes accessed | tf_op | source)
XLA Modules:
  0.0 26.0 jit_solution(13644735563343475877)
XLA Ops:
  0.6 24.5 %shard_map.84 = (bf16[256,512]{1,0:T(8,128)(2,1)S(1)}, bf16[256,512]{1,0:T(8,128)(2,1)S(1)}, bf16[256,512]{1,0:T(8,128)(2,1)S(1)}, f32[32,32]{1,0:T(8,128)S(1)}) custom-call(bf16[256,512]{1,0:T(8,128)(2,1)} %q_hbm.1, bf16[256,512]{1,0:T(8,128)(2,1)} %k_hbm.1, bf16[256,512]{1,0:T(8,128)(2,1)} %v_hbm.1, bf16[256,512]{1,0:T(8,128)(2,1)} %d_hbm.1, f32[32,256]{1,0:T(8,128)} %bitcast.1), custom_call_target="tpu_custom_call" | custom-call | tf_op jit(solution)/shard_map/pallas_call | solution.py:714
  25.1 0.9 %shard_map.85 = (bf16[256,512]{1,0:T(8,128)(2,1)}, bf16[256,512]{1,0:T(8,128)(2,1)}, bf16[256,512]{1,0:T(8,128)(2,1)}, f32[32,32]{1,0:T(8,128)}) custom-call(bf16[256,512]{1,0:T(8,128)(2,1)S(1)} %get-tuple-element.8.refs_0_, bf16[256,512]{1,0:T(8,128)(2,1)S(1)} %get-tuple-element.9.refs_1_, bf16[256,512]{1,0:T(8,128)(2,1)S(1)} %get-tuple-element.10.refs_2_, ...), custom_call_target="tpu_custom_call" | custom-call | tf_op jit(solution)/shard_map/pallas_call | solution.py:753
